TPU v7x, 512 devices: a whole 4x4x16 slice. The times are simulated.
512 devices in a mesh: sp: 128 (over z, x, core), tp: 4 (over y).
Axes of the slice: x: 4, y: 4, z: 16, core: 2. Of those that a mesh axis runs over, the one named last changes fastest.
Arguments:
- tokens: bfloat16 [24576, 2048], P(('sp', 'tp')), may hold values from -7 to 7
- input_norm_gain: float32 [2048], replicated, may hold values from 0.1 to 1.9
- paired_query_weight: bfloat16 [2048, 512], P('sp', 'tp'), may hold values from -16 to 16
- shared_key_weight: bfloat16 [2048, 64], replicated, may hold values from -1 to 1
- shared_value_weight: bfloat16 [2048, 64], replicated, may hold values from -0.125 to 0.125
- recurrent_query_weight: bfloat16 [2048, 1024], P('sp', 'tp'), may hold values from -0.125 to 0.125
- forget_gate_weight: bfloat16 [2048, 1024], P('sp', 'tp'), may hold values from -0.125 to 0.125
- recurrent_value_weight: bfloat16 [2048, 1024], P('sp', 'tp'), may hold values from -0.125 to 0.125
- attention_output_weight: bfloat16 [2048, 512], P('sp', 'tp'), may hold values from -0.15625 to 0.15625
- recurrent_output_weight: bfloat16 [2048, 1024], P('sp', 'tp'), may hold values from -0.15625 to 0.15625
- attention_head_gain: float32 [64], replicated, may hold values from 0.1 to 1.9
- recurrent_head_gain: float32 [128], replicated, may hold values from 0.1 to 1.9
- second_map_weight: float32 [8], P('tp'), may hold values from 0.3 to 0.8
- forget_leak_rate: float32 [1024], P('tp'), may hold values from 2e-05 to 0.05
- extra_log_decay: float32 [24576, 1024], P('sp', 'tp'), may hold values from -1 to 0
- initial_recurrent_state: float32 [8, 128, 128], P('tp'), may hold values from -0.12 to 0.12
Outputs:
- mixer_out: bfloat16 [24576, 2048], P(('sp', 'tp'))
All inputs are finite; a program needn't handle non-finite values.
Results may differ from a plain program's by a relative error of at most 0.014.
Values may be sent and summed in bfloat16 or wider, within the bound.
No kernel may reach another device: no remote copies, remote signals or barrier semaphores. Data moves between devices by JAX's collectives and lax.ppermute only.
A program may use at most 128 MiB of HBM per device.

v0:
```python
import functools
import math

import jax
import jax.numpy as jnp
from jax import lax
from jax.experimental import pallas as pl
from jax.experimental.pallas import tpu as pltpu
from jax.sharding import Mesh
from jax.sharding import PartitionSpec as P


QK_DIM = 32
HEAD_DIM = 64
RECURRENT_WIDTH = 128
REC_SPAN = 64
SP = ("z", "x", "c")
SP_TP = ("z", "x", "c", "tp")
KEY_BLOCK = 512
COLUMN_TILE = 256
PART_ROWS = 80

epsilon = 1e-06


def sent_to_all(x, axis):
    size = lax.axis_size(axis)
    return lax.all_to_all(jnp.broadcast_to(x[None], (size, *x.shape)), axis, 0, 0, tiled=True)


def from_others(x, axis):
    size = lax.axis_size(axis)
    pieces = [x] + [
        lax.ppermute(x, axis, [((k + ahead) % size, k) for k in range(size)])
        for ahead in range(1, size)
    ]
    return jnp.stack(pieces)


def rms_scale(matrix, gain):
    return matrix * lax.rsqrt(jnp.mean(matrix * matrix, axis=-1, keepdims=True) + epsilon) * gain


def project(normed, weight):
    return jnp.dot(normed, weight, preferred_element_type=jnp.float32).astype(jnp.bfloat16)


def whole(shape):
    return pl.BlockSpec(shape, lambda *_: (0,) * len(shape))


def dot_nt(a, b):
    return lax.dot_general(a, b, (((1,), (1,)), ((), ())), preferred_element_type=jnp.float32)


def dot_nn(a, b):
    return jnp.dot(a, b, preferred_element_type=jnp.float32)


def ordered_rows(place_ref, own_ref, other_ref, lanes, ordered):
    n_x, n_z, rows = own_ref.shape[:3]
    core = place_ref[0]
    for x in range(n_x):
        owner = lax.rem(place_ref[1] + x, n_x)
        for z in range(n_z):
            start = (z * n_x + owner) * 2 * rows
            mine = pl.multiple_of(start + core * rows, rows)
            others = pl.multiple_of(start + (1 - core) * rows, rows)
            ordered[pl.ds(mine, rows), :] = own_ref[x, z, :, lanes]
            ordered[pl.ds(others, rows), :] = other_ref[x, z, :, lanes]


def projection_kernel(place_ref, own_ref, other_ref, normed_ref, out_ref, ordered):
    wide = out_ref.shape[1]
    ordered_rows(place_ref, own_ref, other_ref, slice(0, wide), ordered)
    normed = normed_ref[...]
    step = min(wide, 256)
    for k in range(wide // step):
        span = slice(k * step, (k + 1) * step)
        out_ref[:, span] = dot_nn(normed, ordered[:, span]).astype(jnp.bfloat16)


def in_smem():
    return pl.BlockSpec(memory_space=pltpu.SMEM)


def projections(place, own, other, normed, wide):
    tokens, width = normed.shape
    piece = (*own.shape[:3], wide)
    return pl.pallas_call(
        projection_kernel,
        grid=(1,),
        out_shape=jax.ShapeDtypeStruct((tokens, wide), jnp.bfloat16),
        in_specs=[in_smem(), whole(piece), whole(piece), whole(normed.shape)],
        out_specs=whole((tokens, wide)),
        scratch_shapes=[pltpu.VMEM((width, wide), jnp.bfloat16)],
        cost_estimate=pl.CostEstimate(
            flops=2 * tokens * width * wide, bytes_accessed=2 * width * wide, transcendentals=0
        ),
    )(place, own, other, normed)


def one_hot(rows, cols, row_offset, col_offset, count):
    r = lax.broadcasted_iota(jnp.int32, (rows, cols), 0) - row_offset
    c = lax.broadcasted_iota(jnp.int32, (rows, cols), 1) - col_offset
    hit = (r == c) & (r >= 0) & (r < count)
    return jnp.where(hit, 1.0, 0.0).astype(jnp.bfloat16)


def attention_kernel(query_ref, *refs):
    key_value_refs, (out_ref, keys, values_t, lifted_q) = refs[:-4], refs[-4:]
    n_tp, tokens, _ = query_ref.shape
    n_x, n_z, rows, _ = key_value_refs[0].shape
    piece_rows = n_z * rows
    both = 2 * QK_DIM
    twice = one_hot(128, 128, 0, 0, both) + one_hot(128, 128, 0, both, both)
    pick_values = one_hot(PART_ROWS, 128, 0, both, HEAD_DIM)
    ones_row = jnp.where(
        lax.broadcasted_iota(jnp.int32, (PART_ROWS, piece_rows), 0) == HEAD_DIM, 1.0, 0.0
    )
    key_peak = jnp.zeros((8, 128), jnp.float32)
    index = 0
    for ref in key_value_refs:
        for x in range(n_x):
            piece = ref[x].reshape(piece_rows, 128)
            at = index * piece_rows
            doubled = dot_nn(piece, twice)
            keys[at : at + piece_rows, :] = doubled.astype(jnp.bfloat16)
            size = jnp.abs(doubled).reshape(piece_rows // 8, 8, 128)
            key_peak = jnp.maximum(key_peak, jnp.max(size, axis=0))
            values_t[:, at : at + piece_rows] = (
                dot_nt(pick_values, piece) + ones_row
            ).astype(jnp.bfloat16)
            index += 1
    key_count = index * piece_rows
    scale = math.log2(math.e) / math.sqrt(QK_DIM)
    lane = lax.broadcasted_iota(jnp.int32, (tokens, 128), 1) % both
    for tp in range(n_tp):
        scaled = query_ref[tp].astype(jnp.float32) * scale
        high = scaled.astype(jnp.bfloat16)
        low = (scaled - high.astype(jnp.float32)).astype(jnp.bfloat16)
        for head in range(2):
            spread = dot_nn(high, one_hot(128, 128, head * both, 0, both)) + dot_nn(
                low, one_hot(128, 128, head * both, both, both)
            )
            for part in range(2):
                own = (lane >= part * QK_DIM) & (lane < (part + 1) * QK_DIM)
                at = ((tp * 2 + part) * 2 + head) * tokens
                lifted_q[at : at + tokens, :] = jnp.where(own, spread, 0.0).astype(jnp.bfloat16)
    peak_row = jnp.max(key_peak, axis=0, keepdims=True) * 1.02
    bound = dot_nt(
        jnp.broadcast_to(peak_row, (8, 128)).astype(jnp.bfloat16), jnp.abs(lifted_q[...])
    )
    small = jnp.max(bound) < 100.0
    blocks = key_count // KEY_BLOCK
    tiles = lifted_q.shape[0] // COLUMN_TILE
    per_group = tiles // n_tp

    def store(tile, acc, shift):
        group, place = tile // per_group, tile % per_group
        at = pl.multiple_of(place * COLUMN_TILE, COLUMN_TILE)
        row = lax.broadcasted_iota(jnp.int32, (PART_ROWS - HEAD_DIM, COLUMN_TILE), 0)
        tail = jnp.zeros(row.shape, jnp.float32)
        slot = 0
        for rest in (acc[HEAD_DIM : HEAD_DIM + 1, :], shift):
            for _ in range(3):
                high = rest.astype(jnp.bfloat16).astype(jnp.float32)
                tail = jnp.where(row == slot, high, tail)
                rest = rest - high
                slot += 1
        out_ref[group, :HEAD_DIM, pl.ds(at, COLUMN_TILE)] = acc[:HEAD_DIM, :].astype(jnp.bfloat16)
        out_ref[group, HEAD_DIM:, pl.ds(at, COLUMN_TILE)] = tail.astype(jnp.bfloat16)

    @pl.when(small)
    def _():
        @pl.loop(0, n_tp)
        def _(group):
            first = group * per_group

            def queries_of(place):
                start = pl.multiple_of((first + place) * COLUMN_TILE, COLUMN_TILE)
                return lifted_q[pl.ds(start, COLUMN_TILE), :]

            def scores_of(place, b):
                return dot_nt(keys[b * KEY_BLOCK : (b + 1) * KEY_BLOCK, :], queries_of(place))

            visits = [(place, b) for place in range(per_group) for b in range(blocks)]
            scores = scores_of(*visits[0])
            acc = None
            for turn, (place, b) in enumerate(visits):
                ahead = scores_of(*visits[turn + 1]) if turn + 1 < len(visits) else None
                terms = jnp.exp2(scores).astype(jnp.bfloat16)
                product = dot_nn(values_t[:, b * KEY_BLOCK : (b + 1) * KEY_BLOCK], terms)
                acc = product if b == 0 else acc + product
                if b == blocks - 1:
                    store(first + place, acc, jnp.zeros((1, COLUMN_TILE), jnp.float32))
                scores = ahead

    @pl.when(jnp.logical_not(small))
    def _():
        @pl.loop(0, tiles)
        def _(tile):
            start = pl.multiple_of(tile * COLUMN_TILE, COLUMN_TILE)
            q = lifted_q[pl.ds(start, COLUMN_TILE), :]

            def visit(b, state):
                acc, peak = state
                at = pl.multiple_of(b * KEY_BLOCK, KEY_BLOCK)
                scores = dot_nt(keys[pl.ds(at, KEY_BLOCK), :], q)
                new = jnp.maximum(peak, jnp.max(scores, axis=0, keepdims=True))
                terms = jnp.exp2(scores - new).astype(jnp.bfloat16)
                acc = acc * jnp.exp2(peak - new) + dot_nn(
                    values_t[:, pl.ds(at, KEY_BLOCK)], terms
                )
                return acc, new

            acc, peak = lax.fori_loop(
                0,
                blocks,
                visit,
                (
                    jnp.zeros((PART_ROWS, COLUMN_TILE), jnp.float32),
                    jnp.full((1, COLUMN_TILE), -3e38, jnp.float32),
                ),
            )
            store(tile, acc, peak)


def attention(queries, sources, first_lane_block, piece_count):
    n_tp, tokens, _ = queries.shape
    n_x, n_z, rows, _ = sources[0].shape
    key_count = n_x * n_z * rows * piece_count * len(sources)
    columns = n_tp * tokens * 4

    def piece(k):
        return pl.BlockSpec((n_x, n_z, rows, 128), lambda *_: (0, 0, 0, first_lane_block + k))

    return pl.pallas_call(
        attention_kernel,
        grid=(1,),
        out_shape=jax.ShapeDtypeStruct((n_tp, PART_ROWS, tokens * 4), jnp.bfloat16),
        in_specs=[whole(queries.shape)] + [piece(k) for k in range(piece_count)] * len(sources),
        out_specs=whole((n_tp, PART_ROWS, tokens * 4)),
        scratch_shapes=[
            pltpu.VMEM((key_count, 128), jnp.bfloat16),
            pltpu.VMEM((PART_ROWS, key_count), jnp.bfloat16),
            pltpu.VMEM((columns, 128), jnp.bfloat16),
        ],
        cost_estimate=pl.CostEstimate(
            flops=2 * columns * key_count * 512,
            bytes_accessed=2 * key_count * 128,
            transcendentals=columns * key_count,
        ),
        name="attention",
    )(queries, *[source for source in sources for _ in range(piece_count)])


def in_three(matrix):
    high = matrix.astype(jnp.bfloat16)
    rest = matrix - high.astype(jnp.float32)
    middle = rest.astype(jnp.bfloat16)
    return high, middle, (rest - middle.astype(jnp.float32)).astype(jnp.bfloat16)


def recurrence_kernel(raw_ref, leak_ref, extra_ref, local_ref, lifted_ref, sent_ref, held):
    rows, wide = extra_ref.shape
    heads = wide // RECURRENT_WIDTH
    raw_query = raw_ref[:, :wide].astype(jnp.float32)
    raw_gate = raw_ref[:, wide : 2 * wide].astype(jnp.float32)
    query = raw_query * jax.nn.sigmoid(raw_query)
    inflow = leak_ref[...] * (1.0 - jax.nn.sigmoid(raw_gate))
    log_decay = jnp.log(1.0 - inflow) + extra_ref[...]
    lower = lax.broadcasted_iota(jnp.int32, (REC_SPAN, REC_SPAN), 0) >= lax.broadcasted_iota(
        jnp.int32, (REC_SPAN, REC_SPAN), 1
    )
    triangle = jnp.where(lower, 1.0, 0.0).astype(jnp.bfloat16)
    offset = jnp.zeros((1, wide), jnp.float32)
    states = [jnp.zeros((RECURRENT_WIDTH, RECURRENT_WIDTH), jnp.float32)] * heads
    for span in range(rows // REC_SPAN):
        part = slice(span * REC_SPAN, (span + 1) * REC_SPAN)
        running = sum(dot_nn(triangle, term) for term in in_three(log_decay[part]))
        final = running[REC_SPAN - 1 :, :]
        decayed = query[part] * jnp.exp(running)
        lifted = query[part] * jnp.exp(offset + running)
        opened = (inflow[part] * jnp.exp(-running)).astype(jnp.bfloat16)
        closing = (inflow[part] * jnp.exp(final - running)).astype(jnp.bfloat16)
        kept = jnp.exp(final)
        offset = offset + final
        for head in range(heads):
            lanes = slice(head * RECURRENT_WIDTH, (head + 1) * RECURRENT_WIDTH)
            values = raw_ref[part, 2 * wide + lanes.start : 2 * wide + lanes.stop]
            mine = decayed[:, lanes].astype(jnp.bfloat16)
            within = jnp.where(lower, dot_nt(mine, opened[:, lanes]), 0.0)
            local = dot_nn(within.astype(jnp.bfloat16), values)
            if span > 0:
                local = local + dot_nt(mine, states[head].astype(jnp.bfloat16))
            local_ref[head, part, :] = local
            lifted_ref[head, part, :] = lifted[:, lanes].astype(jnp.bfloat16)
            states[head] = kept[:, lanes] * states[head] + lax.dot_general(
                values, closing[:, lanes], (((0,), (0,)), ((), ())),
                preferred_element_type=jnp.float32,
            )
    held[heads * RECURRENT_WIDTH :, :] = jnp.zeros((8, RECURRENT_WIDTH), jnp.float32)
    for head in range(heads):
        held[head * RECURRENT_WIDTH : (head + 1) * RECURRENT_WIDTH, :] = states[head]
    members = sent_ref.shape[0]
    state_row = lax.broadcasted_iota(jnp.int32, (4, RECURRENT_WIDTH), 0) < 2
    decays = jnp.exp(offset)
    for k in range(members):
        head = k * heads // members
        decay = decays[:, head * RECURRENT_WIDTH : (head + 1) * RECURRENT_WIDTH]
        sent_ref[k] = jnp.where(state_row, held[2 * k : 2 * k + 4, :], decay).astype(jnp.bfloat16)


def local_recurrence(raw, leak, extra, members):
    rows, wide = extra.shape
    heads = wide // RECURRENT_WIDTH
    by_head = (heads, rows, RECURRENT_WIDTH)
    sent = (members, 4, RECURRENT_WIDTH)
    return pl.pallas_call(
        recurrence_kernel,
        grid=(1,),
        out_shape=(
            jax.ShapeDtypeStruct(by_head, jnp.float32),
            jax.ShapeDtypeStruct(by_head, jnp.bfloat16),
            jax.ShapeDtypeStruct(sent, jnp.bfloat16),
        ),
        in_specs=[whole(raw.shape), whole(leak.shape), whole(extra.shape)],
        out_specs=(whole(by_head), whole(by_head), whole(sent)),
        scratch_shapes=[pltpu.VMEM((heads * RECURRENT_WIDTH + 8, RECURRENT_WIDTH), jnp.float32)],
        cost_estimate=pl.CostEstimate(
            flops=2 * rows * wide * 1024, bytes_accessed=8 * rows * wide, transcendentals=0
        ),
        name="recurrence",
    )(raw, leak, extra)


def chain_kernel(first_ref, pieces_ref, out_ref):
    def visit(k, state):
        out_ref[k] = state.astype(jnp.bfloat16)
        piece = pieces_ref[k].astype(jnp.float32)
        return piece[2:3, :] * state + piece[0:2, :]

    lax.fori_loop(0, pieces_ref.shape[0], visit, first_ref[...], unroll=8)


def chained(first, pieces):
    count = pieces.shape[0]
    return pl.pallas_call(
        chain_kernel,
        grid=(1,),
        out_shape=jax.ShapeDtypeStruct((count, 2, 128), jnp.bfloat16),
        in_specs=[whole(first.shape), whole(pieces.shape)],
        out_specs=whole((count, 2, 128)),
        name="chained",
    )(first, pieces)


def output_kernel(
    place_ref,
    second_ref,
    parts_ref,
    attn_gain_ref,
    local_ref,
    lifted_ref,
    state_ref,
    rec_gain_ref,
    own_ref,
    other_ref,
    out_ref,
    ordered,
):
    n_lanes = ordered.shape[1]
    first = own_ref.shape[3] - n_lanes
    ordered_rows(place_ref, own_ref, other_ref, slice(first, first + n_lanes), ordered)
    members = parts_ref.shape[0]
    tokens = local_ref.shape[1]
    columns = parts_ref.shape[2]
    half = columns // 2

    def joined(k, row):
        lines = parts_ref[k, HEAD_DIM:, :].astype(jnp.float32)
        return lines[row : row + 1] + lines[row + 1 : row + 2] + lines[row + 2 : row + 3]

    shifts = [joined(k, 3) for k in range(members)]
    top = functools.reduce(jnp.maximum, shifts)
    weighted = jnp.zeros((HEAD_DIM, columns), jnp.float32)
    totals = jnp.zeros((1, columns), jnp.float32)
    for k in range(members):
        factor = jnp.exp2(shifts[k] - top)
        weighted = weighted + parts_ref[k, :HEAD_DIM, :].astype(jnp.float32) * factor
        totals = totals + joined(k, 0) * factor
    ratio = weighted / totals
    head_of = lax.broadcasted_iota(jnp.int32, (1, half), 1) >= tokens
    second = jnp.where(head_of, second_ref[1], second_ref[0])
    blended = ratio[:, :half] - second * ratio[:, half:]
    scale = lax.rsqrt(jnp.mean(blended * blended, axis=0, keepdims=True) + epsilon)
    hidden_t = blended * scale * attn_gain_ref[...]
    turned = jnp.concatenate([hidden_t, hidden_t], axis=0).T
    lane = lax.broadcasted_iota(jnp.int32, (tokens, 2 * HEAD_DIM), 1)
    hidden = [jnp.where(lane < HEAD_DIM, turned[:tokens], turned[tokens:]).astype(jnp.bfloat16)]
    for head in range(local_ref.shape[0]):
        rec = local_ref[head] + dot_nt(lifted_ref[head], state_ref[head])
        scale = lax.rsqrt(jnp.mean(rec * rec, axis=1, keepdims=True) + epsilon)
        hidden.append((rec * scale * rec_gain_ref[...]).astype(jnp.bfloat16))
    hidden = jnp.concatenate(hidden, axis=1)
    step = 512
    for k in range(out_ref.shape[1] // step):
        span = slice(k * step, (k + 1) * step)
        out_ref[:, span] = dot_nt(hidden, ordered[span, :]).astype(jnp.bfloat16)


def output_partial(place, second, parts, attn_gain, local, lifted, state, rec_gain, own, other):
    heads, tokens, width = local.shape
    n_x, n_z, rows, _ = own.shape
    model = n_x * n_z * rows * 2
    mixed = parts.shape[2] // (2 * tokens) * HEAD_DIM + heads * width
    arrays = (parts, attn_gain, local, lifted, state, rec_gain, own, other)
    return pl.pallas_call(
        output_kernel,
        grid=(1,),
        out_shape=jax.ShapeDtypeStruct((tokens, model), jnp.bfloat16),
        in_specs=[in_smem(), in_smem()] + [whole(a.shape) for a in arrays],
        out_specs=whole((tokens, model)),
        scratch_shapes=[pltpu.VMEM((model, mixed), jnp.bfloat16)],
        cost_estimate=pl.CostEstimate(
            flops=2 * tokens * model * mixed, bytes_accessed=2 * model * mixed, transcendentals=0
        ),
        name="output_partial",
    )(place, second, *arrays)


def body(
    tokens,
    input_norm_gain,
    paired_query_weight,
    shared_key_weight,
    shared_value_weight,
    recurrent_query_weight,
    forget_gate_weight,
    recurrent_value_weight,
    attention_output_weight,
    recurrent_output_weight,
    attention_head_gain,
    recurrent_head_gain,
    second_map_weight,
    forget_leak_rate,
    extra_log_decay,
    initial_recurrent_state,
):
    place = jnp.stack([lax.axis_index("c"), lax.axis_index("x")]).astype(jnp.int32)
    own_normed = rms_scale(tokens.astype(jnp.float32), input_norm_gain).astype(jnp.bfloat16)
    own_rows = own_normed.shape[0]
    first_payload = jnp.concatenate(
        [recurrent_query_weight, forget_gate_weight, recurrent_value_weight], axis=1
    )
    key_value = project(
        own_normed, jnp.concatenate([shared_key_weight, shared_value_weight], axis=1)
    )
    rows = paired_query_weight.shape[0]
    narrow = paired_query_weight.shape[1]
    kv_pieces = own_rows // rows
    second_payload = jnp.concatenate(
        [paired_query_weight]
        + [key_value[k * rows : (k + 1) * rows] for k in range(kv_pieces)]
        + [attention_output_weight, recurrent_output_weight],
        axis=1,
    )
    swap = [(0, 1), (1, 0)]
    first_z = sent_to_all(first_payload, "z")
    normed = lax.all_gather(own_normed, "tp", axis=0, tiled=True)
    second_payload, first_z, normed = lax.optimization_barrier((second_payload, first_z, normed))
    second_z = sent_to_all(second_payload, "z")
    first_own = from_others(first_z, "x")
    first_other = lax.ppermute(first_own, "c", swap)
    recur = first_payload.shape[1]
    recur_raw = projections(place, first_own, first_other, normed, recur)
    local_output, lifted, sent = local_recurrence(
        recur_raw, forget_leak_rate[None, :], extra_log_decay, lax.axis_size(SP)
    )
    sent, second_z = lax.optimization_barrier((sent, second_z))
    arrived = lax.all_to_all(sent, SP, 0, 0, tiled=True)
    second_own = from_others(second_z, "x")
    second_other = lax.ppermute(second_own, "c", swap)
    first = lax.dynamic_index_in_dim(
        initial_recurrent_state.transpose(0, 2, 1).reshape(sent.shape[0], 2, 128),
        lax.axis_index(SP),
        0,
        False,
    )
    before = chained(first, arrived)
    incoming_state = lax.all_to_all(before, SP, 0, 0, tiled=True)
    incoming_state = incoming_state.reshape(initial_recurrent_state.shape)
    queries = projections(place, second_own, second_other, normed, narrow)
    all_queries = lax.all_gather(queries, "tp", axis=0)
    parts = attention(all_queries, (second_own, second_other), narrow // 128, kv_pieces)
    landed_parts = lax.all_to_all(parts, "tp", 0, 0, tiled=True)
    partial = output_partial(
        place,
        second_map_weight,
        landed_parts,
        attention_head_gain[:, None],
        local_output,
        lifted,
        incoming_state,
        recurrent_head_gain[None, :],
        second_own,
        second_other,
    )
    size = lax.axis_size("tp")
    blocks = partial.reshape(size, own_rows, partial.shape[1])
    landed = lax.all_to_all(blocks, "tp", 0, 0, tiled=True)
    return landed.astype(jnp.float32).sum(axis=0).astype(jnp.bfloat16)


def solution(mesh):
    torus = Mesh(mesh.devices.reshape(16, 4, 2, mesh.shape["tp"]), SP_TP)
    placed = (
        P(SP_TP, None),
        P(),
        P(SP, "tp"),
        P(),
        P(),
        P(SP, "tp"),
        P(SP, "tp"),
        P(SP, "tp"),
        P(SP, "tp"),
        P(SP, "tp"),
        P(),
        P(),
        P("tp"),
        P("tp"),
        P(SP, "tp"),
        P("tp", None, None),
    )

    return jax.shard_map(
        body, mesh=torus, in_specs=placed, out_specs=P(SP_TP, None), check_vma=False
    )
```

profile of v0, /device:TPU:2, one launch (start us, length us, event | category | flops | bytes accessed | tf_op | source)
XLA Modules:
  0.0 276.1 jit_solution(11851243947255920825)
XLA Ops:
  1.6 15.2 %all-to-all-start = ((bf16[16,16,768]{2,1,0:T(8,128)(2,1)}), bf16[16,16,768]{2,1,0:T(8,128)(2,1)S(1)}, u32[]{:S(2)}, u32[]{:S(2)}) async-start(bf16[16,16,768]{2,1,0:T(8,128)(2,1)} %broadcast_in_dim.10), calls=%async_computation | async-start | bytes 786432 | tf_op jit(solution)/shard_map/all_to_all | solution.py:28
  19.4 14.6 %all_gather.9.normed_ref = bf16[192,2048]{1,0:T(8,128)(2,1)} all-gather(bf16[48,2048]{1,0:T(8,128)(2,1)S(1)} %fusion.5), channel_id=1, replica_groups=mesh['z'=16,'x'=4,'c'=2,'tp'=4] {'tp'}, dimensions={0}, use_global_device_ids=true | all-gather | bytes 983040 | tf_op jit(solution)/shard_map/all_gather | solution.py:471
  34.0 6.6 %all-to-all-done = bf16[16,16,768]{2,1,0:T(8,128)(2,1)S(1)} async-done(((bf16[16,16,768]{2,1,0:T(8,128)(2,1)}), bf16[16,16,768]{2,1,0:T(8,128)(2,1)S(1)}, u32[]{:S(2)}, u32[]{:S(2)}) %all-to-all-start) | async-done | bytes 393248 | tf_op jit(solution)/shard_map/all_to_all | solution.py:28
  40.6 3.4 %collective-permute-start.2 = (bf16[16,16,768]{2,1,0:T(8,128)(2,1)S(1)}, bf16[16,16,768]{2,1,0:T(8,128)(2,1)S(1)}, u32[]{:S(2)}, u32[]{:S(2)}) collective-permute-start(bf16[16,16,768]{2,1,0:T(8,128)(2,1)S(1)} %all-to-all-done), channel_id=1, source_target_pairs={{24,0},{0,8},{8,16},{16,24},{25,1},{1,9},{9,17},{17,25},{26,2},{2,... | collective-permute-start | bytes 1179656 | tf_op jit(solution)/shard_map/ppermute | solution.py:34
  44.0 3.0 %collective-permute-start.1 = (bf16[16,16,768]{2,1,0:T(8,128)(2,1)S(1)}, bf16[16,16,768]{2,1,0:T(8,128)(2,1)S(1)}, u32[]{:S(2)}, u32[]{:S(2)}) collective-permute-start(bf16[16,16,768]{2,1,0:T(8,128)(2,1)S(1)} %all-to-all-done), channel_id=1, source_target_pairs={{16,0},{24,8},{0,16},{8,24},{17,1},{25,9},{1,17},{9,25},{18,2},{26... | collective-permute-start | bytes 1179656 | tf_op jit(solution)/shard_map/ppermute | solution.py:34
  47.0 4.1 %collective-permute-start = (bf16[16,16,768]{2,1,0:T(8,128)(2,1)S(1)}, bf16[16,16,768]{2,1,0:T(8,128)(2,1)S(1)}, u32[]{:S(2)}, u32[]{:S(2)}) collective-permute-start(bf16[16,16,768]{2,1,0:T(8,128)(2,1)S(1)} %all-to-all-done), channel_id=1, source_target_pairs={{8,0},{16,8},{24,16},{0,24},{9,1},{17,9},{25,17},{1,25},{10,2},{18... | collective-permute-start | bytes 1179656 | tf_op jit(solution)/shard_map/ppermute | solution.py:34
  51.9 6.0 %all-to-all-start.1 = ((bf16[16,16,896]{2,1,0:T(8,128)(2,1)}), bf16[16,16,896]{2,1,0:T(8,128)(2,1)S(1)}, u32[]{:S(2)}, u32[]{:S(2)}) async-start(bf16[16,16,896]{2,1,0:T(8,128)(2,1)} %broadcast_in_dim.12), calls=%async_computation.1 | async-start | bytes 917504 | tf_op jit(solution)/shard_map/all_to_all | solution.py:28
  64.9 2.9 %collective-permute-done.3.other_ref = bf16[4,16,16,768]{3,2,1,0:T(8,128)(2,1)} collective-permute-done((bf16[4,16,16,768]{3,2,1,0:T(8,128)(2,1)S(1)}, bf16[4,16,16,768]{3,2,1,0:T(8,128)(2,1)}, u32[]{:S(2)}, u32[]{:S(2)}) %collective-permute-start.3) | collective-permute-done | bytes 1572896 | tf_op jit(solution)/shard_map/ppermute | solution.py:475
  67.8 3.8 %shard_map.154.raw_ref = bf16[192,768]{1,0:T(8,128)(2,1)} custom-call(s32[2]{0:T(128)} %pad_add_fusion.place_ref, bf16[4,16,16,768]{3,2,1,0:T(8,128)(2,1)} %copy-done.1, bf16[4,16,16,768]{3,2,1,0:T(8,128)(2,1)} %collective-permute-done.3.other_ref, bf16[192,2048]{1,0:T(8,128)(2,1)} %all_gather.9.normed_ref), custom_call_target="tpu_custom_call" | custom-call | flops 603979776 | bytes 3145728 | tf_op jit(solution)/shard_map/pallas_call | solution.py:90
  71.6 3.0 %recurrence.1 = (f32[2,192,128]{2,1,0:T(8,128)}, bf16[2,192,128]{2,1,0:T(8,128)(2,1)}, bf16[128,4,128]{2,1,0:T(4,128)(2,1)}) custom-call(bf16[192,768]{1,0:T(8,128)(2,1)} %shard_map.154.raw_ref, f32[1,256]{1,0:T(1,128)} %bitcast.34, f32[192,256]{1,0:T(8,128)} %extra_ref.1), custom_call_target="tpu_custom_call" | custom-call | flops 100663296 | bytes 393216 | tf_op jit(solution)/shard_map/recurrence/pallas_call | solution.py:320
  74.6 7.7 %all-to-all-done.1 = bf16[16,16,896]{2,1,0:T(8,128)(2,1)S(1)} async-done(((bf16[16,16,896]{2,1,0:T(8,128)(2,1)}), bf16[16,16,896]{2,1,0:T(8,128)(2,1)S(1)}, u32[]{:S(2)}, u32[]{:S(2)}) %all-to-all-start.1) | async-done | bytes 458784 | tf_op jit(solution)/shard_map/all_to_all | solution.py:28
  84.3 5.4 %collective-permute-start.5 = (bf16[16,16,896]{2,1,0:T(8,128)(2,1)S(1)}, bf16[16,16,896]{2,1,0:T(8,128)(2,1)S(1)}, u32[]{:S(2)}, u32[]{:S(2)}) collective-permute-start(bf16[16,16,896]{2,1,0:T(8,128)(2,1)S(1)} %all-to-all-done.1), channel_id=1, source_target_pairs={{16,0},{24,8},{0,16},{8,24},{17,1},{25,9},{1,17},{9,25},{18,2},{26... | collective-permute-start | bytes 1376264 | tf_op jit(solution)/shard_map/ppermute | solution.py:34
  91.6 4.1 %collective-permute-done.6 = bf16[16,16,896]{2,1,0:T(8,128)(2,1)S(1)} collective-permute-done((bf16[16,16,896]{2,1,0:T(8,128)(2,1)S(1)}, bf16[16,16,896]{2,1,0:T(8,128)(2,1)S(1)}, u32[]{:S(2)}, u32[]{:S(2)}) %collective-permute-start.6) | collective-permute-done | bytes 458784 | tf_op jit(solution)/shard_map/ppermute | solution.py:34
  95.7 3.5 %collective-permute-done.5 = bf16[16,16,896]{2,1,0:T(8,128)(2,1)S(1)} collective-permute-done((bf16[16,16,896]{2,1,0:T(8,128)(2,1)S(1)}, bf16[16,16,896]{2,1,0:T(8,128)(2,1)S(1)}, u32[]{:S(2)}, u32[]{:S(2)}) %collective-permute-start.5) | collective-permute-done | bytes 458784 | tf_op jit(solution)/shard_map/ppermute | solution.py:34
  99.2 4.8 %collective-permute-done.4 = bf16[16,16,896]{2,1,0:T(8,128)(2,1)S(1)} collective-permute-done((bf16[16,16,896]{2,1,0:T(8,128)(2,1)S(1)}, bf16[16,16,896]{2,1,0:T(8,128)(2,1)S(1)}, u32[]{:S(2)}, u32[]{:S(2)}) %collective-permute-start.4) | collective-permute-done | bytes 458784 | tf_op jit(solution)/shard_map/ppermute | solution.py:34
  106.2 17.3 %all-to-all-start.3 = ((bf16[128,4,128]{2,1,0:T(4,128)(2,1)}), bf16[128,4,128]{2,1,0:T(4,128)(2,1)S(1)}, u32[]{:S(2)}, u32[]{:S(2)}) async-start(bf16[128,4,128]{2,1,0:T(4,128)(2,1)} %get-tuple-element.20), calls=%async_computation.3 | async-start | bytes 262144 | tf_op jit(solution)/shard_map/all_to_all | solution.py:482
  124.3 15.5 %all-to-all-done.3.pieces_ref = bf16[128,4,128]{2,1,0:T(4,128)(2,1)S(1)} async-done(((bf16[128,4,128]{2,1,0:T(4,128)(2,1)}), bf16[128,4,128]{2,1,0:T(4,128)(2,1)S(1)}, u32[]{:S(2)}, u32[]{:S(2)}) %all-to-all-start.3) | async-done | bytes 131104 | tf_op jit(solution)/shard_map/all_to_all | solution.py:482
  142.3 7.0 %all-to-all-start.4 = ((bf16[128,2,128]{2,1,0:T(2,128)(2,1)}), bf16[128,2,128]{2,1,0:T(2,128)(2,1)S(1)}, u32[]{:S(2)}, u32[]{:S(2)}) async-start(bf16[128,2,128]{2,1,0:T(2,128)(2,1)} %chained.1), calls=%async_computation.4 | async-start | bytes 131072 | tf_op jit(solution)/shard_map/all_to_all | solution.py:492
  151.8 14.4 %all-gather = bf16[768,128]{1,0:T(8,128)(2,1)} all-gather(bf16[192,128]{1,0:T(8,128)(2,1)} %shard_map.155), channel_id=2, replica_groups=mesh['z'=16,'x'=4,'c'=2,'tp'=4] {'tp'}, dimensions={0}, use_global_device_ids=true | all-gather | bytes 245760 | tf_op jit(solution)/shard_map/all_gather | solution.py:495
  166.2 79.7 %attention.1 = bf16[4,80,768]{2,1,0:T(8,128)(2,1)} custom-call(bf16[4,192,128]{2,1,0:T(8,128)(2,1)} %bitcast.32, bf16[4,16,16,896]{3,2,1,0:T(8,128)(2,1)} %copy-done, bf16[4,16,16,896]{3,2,1,0:T(8,128)(2,1)} %copy-done, bf16[4,16,16,896]{3,2,1,0:T(8,128)(2,1)} %copy-done, bf16[4,16,16,896]{3,2,1,0:T(8,128)(2,1)} %collective-permute-done.7.other_ref.refs_3_.refs_4_.refs_5_, ...), custom_call_target="tpu_custom_call" | custom-call | flops 19327352832 | bytes 1572864 | tf_op jit(solution)/shard_map/attention/pallas_call | solution.py:238
  245.9 3.5 %all-to-all-start.2 = ((bf16[4,80,768]{2,1,0:T(8,128)(2,1)}), bf16[4,80,768]{2,1,0:T(8,128)(2,1)S(1)}, u32[]{:S(2)}, u32[]{:S(2)}) async-start(bf16[4,80,768]{2,1,0:T(8,128)(2,1)} %attention.1), calls=%async_computation.2 | async-start | bytes 983040 | tf_op jit(solution)/shard_map/all_to_all | solution.py:497
  250.1 7.2 %all-to-all-done.2.parts_ref = bf16[4,80,768]{2,1,0:T(8,128)(2,1)S(1)} async-done(((bf16[4,80,768]{2,1,0:T(8,128)(2,1)}), bf16[4,80,768]{2,1,0:T(8,128)(2,1)S(1)}, u32[]{:S(2)}, u32[]{:S(2)}) %all-to-all-start.2) | async-done | bytes 491552 | tf_op jit(solution)/shard_map/all_to_all | solution.py:497
  258.0 4.3 %output_partial.1 = bf16[192,2048]{1,0:T(8,128)(2,1)} custom-call(s32[2]{0:T(128)} %pad_add_fusion.place_ref, f32[2]{0:T(128)} %second_ref.1, bf16[4,80,768]{2,1,0:T(8,128)(2,1)} %copy-done.2, f32[64,1]{1,0:T(8,128)} %copy.19.attn_gain_ref, f32[2,192,128]{2,1,0:T(8,128)} %get-tuple-element.18.local_ref, bf16[2,192,128]{2,1,0:T(8,128)(2,1)} %get-tuple-element.19.lifted_ref, ...), custom_call_target="tpu_custom_call" | custom-call | flops 301989888 | bytes 1572864 | tf_op jit(solution)/shard_map/output_partial/pallas_call | solution.py:419
  262.4 12.9 %all_to_all.30 = bf16[4,48,2048]{2,1,0:T(8,128)(2,1)S(1)} all-to-all(bf16[4,48,2048]{2,1,0:T(8,128)(2,1)} %bitcast.22), channel_id=1, replica_groups=mesh['z'=16,'x'=4,'c'=2,'tp'=4] {'tp'}, dimensions={0} | all-to-all | bytes 1572864 | tf_op jit(solution)/shard_map/all_to_all | solution.py:512
  (57 shorter events, 25.9 us)
Async XLA Ops:
  0.0 18.9 %copy-start.8 = (bf16[16,128]{1,0:T(8,128)(2,1)S(1)}, bf16[16,128]{1,0:T(8,128)(2,1)}, u32[]{:S(2)}) copy-start(bf16[16,128]{1,0:T(8,128)(2,1)} %param.18) | copy-start | bytes 12292
  0.0 19.0 %copy-start.11 = (bf16[2048,64]{0,1:T(8,128)(2,1)S(1)}, bf16[2048,64]{0,1:T(8,128)(2,1)}, u32[]{:S(2)}) copy-start(bf16[2048,64]{0,1:T(8,128)(2,1)} %param.20) | copy-start | bytes 786436
  0.0 19.0 %copy-start.12 = (bf16[2048,64]{0,1:T(8,128)(2,1)S(1)}, bf16[2048,64]{0,1:T(8,128)(2,1)}, u32[]{:S(2)}) copy-start(bf16[2048,64]{0,1:T(8,128)(2,1)} %param.19) | copy-start | bytes 786436
  0.0 19.3 %copy-start.9 = (bf16[16,128]{1,0:T(8,128)(2,1)S(1)}, bf16[16,128]{1,0:T(8,128)(2,1)}, u32[]{:S(2)}) copy-start(bf16[16,128]{1,0:T(8,128)(2,1)} %param.24) | copy-start | bytes 12292
  0.0 19.3 %copy-start.7 = (bf16[16,256]{1,0:T(8,128)(2,1)S(1)}, bf16[16,256]{1,0:T(8,128)(2,1)}, u32[]{:S(2)}) copy-start(bf16[16,256]{1,0:T(8,128)(2,1)} %param.25) | copy-start | bytes 24580
  1.6 39.0 %all-to-all-start = ((bf16[16,16,768]{2,1,0:T(8,128)(2,1)}), bf16[16,16,768]{2,1,0:T(8,128)(2,1)S(1)}, u32[]{:S(2)}, u32[]{:S(2)}) async-start(bf16[16,16,768]{2,1,0:T(8,128)(2,1)} %broadcast_in_dim.10), calls=%async_computation | async-start | bytes 786432 | tf_op jit(solution)/shard_map/all_to_all | solution.py:28
  40.6 17.3 %collective-permute-start.2 = (bf16[16,16,768]{2,1,0:T(8,128)(2,1)S(1)}, bf16[16,16,768]{2,1,0:T(8,128)(2,1)S(1)}, u32[]{:S(2)}, u32[]{:S(2)}) collective-permute-start(bf16[16,16,768]{2,1,0:T(8,128)(2,1)S(1)} %all-to-all-done), channel_id=1, source_target_pairs={{24,0},{0,8},{8,16},{16,24},{25,1},{1,9},{9,17},{17,25},{26,2},{2,... | collective-permute-start | bytes 1179656 | tf_op jit(solution)/shard_map/ppermute | solution.py:34
  44.0 13.9 %collective-permute-start.1 = (bf16[16,16,768]{2,1,0:T(8,128)(2,1)S(1)}, bf16[16,16,768]{2,1,0:T(8,128)(2,1)S(1)}, u32[]{:S(2)}, u32[]{:S(2)}) collective-permute-start(bf16[16,16,768]{2,1,0:T(8,128)(2,1)S(1)} %all-to-all-done), channel_id=1, source_target_pairs={{16,0},{24,8},{0,16},{8,24},{17,1},{25,9},{1,17},{9,25},{18,2},{26... | collective-permute-start | bytes 1179656 | tf_op jit(solution)/shard_map/ppermute | solution.py:34
  47.0 13.4 %collective-permute-start = (bf16[16,16,768]{2,1,0:T(8,128)(2,1)S(1)}, bf16[16,16,768]{2,1,0:T(8,128)(2,1)S(1)}, u32[]{:S(2)}, u32[]{:S(2)}) collective-permute-start(bf16[16,16,768]{2,1,0:T(8,128)(2,1)S(1)} %all-to-all-done), channel_id=1, source_target_pairs={{8,0},{16,8},{24,16},{0,24},{9,1},{17,9},{25,17},{1,25},{10,2},{18... | collective-permute-start | bytes 1179656 | tf_op jit(solution)/shard_map/ppermute | solution.py:34
  51.9 30.5 %all-to-all-start.1 = ((bf16[16,16,896]{2,1,0:T(8,128)(2,1)}), bf16[16,16,896]{2,1,0:T(8,128)(2,1)S(1)}, u32[]{:S(2)}, u32[]{:S(2)}) async-start(bf16[16,16,896]{2,1,0:T(8,128)(2,1)} %broadcast_in_dim.12), calls=%async_computation.1 | async-start | bytes 917504 | tf_op jit(solution)/shard_map/all_to_all | solution.py:28
  62.4 5.4 %copy-start.1 = (bf16[4,16,16,768]{3,2,1,0:T(8,128)(2,1)}, bf16[4,16,16,768]{3,2,1,0:T(8,128)(2,1)S(1)}, u32[]{:S(2)}) copy-start(bf16[4,16,16,768]{3,2,1,0:T(8,128)(2,1)S(1)} %pad_maximum_fusion.1.own_ref) | copy-start | bytes 4718596
  62.4 5.4 %collective-permute-start.3 = (bf16[4,16,16,768]{3,2,1,0:T(8,128)(2,1)S(1)}, bf16[4,16,16,768]{3,2,1,0:T(8,128)(2,1)}, u32[]{:S(2)}, u32[]{:S(2)}) collective-permute-start(bf16[4,16,16,768]{3,2,1,0:T(8,128)(2,1)S(1)} %pad_maximum_fusion.1.own_ref), channel_id=1, source_target_pairs={{0,4},{4,0},{1,5},{5,1},{2,6},{6,2},{3,7},{7,3},{8,12},{12,8},{9,1... | collective-permute-start | bytes 4718600 | tf_op jit(solution)/shard_map/ppermute | solution.py:475
  82.4 13.3 %collective-permute-start.6 = (bf16[16,16,896]{2,1,0:T(8,128)(2,1)S(1)}, bf16[16,16,896]{2,1,0:T(8,128)(2,1)S(1)}, u32[]{:S(2)}, u32[]{:S(2)}) collective-permute-start(bf16[16,16,896]{2,1,0:T(8,128)(2,1)S(1)} %all-to-all-done.1), channel_id=1, source_target_pairs={{24,0},{0,8},{8,16},{16,24},{25,1},{1,9},{9,17},{17,25},{26,2},{2,... | collective-permute-start | bytes 1376264 | tf_op jit(solution)/shard_map/ppermute | solution.py:34
  84.3 15.0 %collective-permute-start.5 = (bf16[16,16,896]{2,1,0:T(8,128)(2,1)S(1)}, bf16[16,16,896]{2,1,0:T(8,128)(2,1)S(1)}, u32[]{:S(2)}, u32[]{:S(2)}) collective-permute-start(bf16[16,16,896]{2,1,0:T(8,128)(2,1)S(1)} %all-to-all-done.1), channel_id=1, source_target_pairs={{16,0},{24,8},{0,16},{8,24},{17,1},{25,9},{1,17},{9,25},{18,2},{26... | collective-permute-start | bytes 1376264 | tf_op jit(solution)/shard_map/ppermute | solution.py:34
  89.7 14.4 %collective-permute-start.4 = (bf16[16,16,896]{2,1,0:T(8,128)(2,1)S(1)}, bf16[16,16,896]{2,1,0:T(8,128)(2,1)S(1)}, u32[]{:S(2)}, u32[]{:S(2)}) collective-permute-start(bf16[16,16,896]{2,1,0:T(8,128)(2,1)S(1)} %all-to-all-done.1), channel_id=1, source_target_pairs={{8,0},{16,8},{24,16},{0,24},{9,1},{17,9},{25,17},{1,25},{10,2},{18... | collective-permute-start | bytes 1376264 | tf_op jit(solution)/shard_map/ppermute | solution.py:34
  104.0 19.6 %copy-start.6 = (f32[2,128,128]{2,1,0:T(8,128)S(1)}, f32[2,128,128]{2,1,0:T(8,128)}, u32[]{:S(2)}) copy-start(f32[2,128,128]{2,1,0:T(8,128)} %param.31) | copy-start | bytes 393220
  104.3 45.0 %copy-start = (bf16[4,16,16,896]{3,2,1,0:T(8,128)(2,1)}, bf16[4,16,16,896]{3,2,1,0:T(8,128)(2,1)S(1)}, u32[]{:S(2)}) copy-start(bf16[4,16,16,896]{3,2,1,0:T(8,128)(2,1)S(1)} %pad_maximum_fusion.own_ref.refs_0_.refs_1_.refs_2_) | copy-start | bytes 5505028
  104.3 45.0 %collective-permute-start.7 = (bf16[4,16,16,896]{3,2,1,0:T(8,128)(2,1)S(1)}, bf16[4,16,16,896]{3,2,1,0:T(8,128)(2,1)}, u32[]{:S(2)}, u32[]{:S(2)}) collective-permute-start(bf16[4,16,16,896]{3,2,1,0:T(8,128)(2,1)S(1)} %pad_maximum_fusion.own_ref.refs_0_.refs_1_.refs_2_), channel_id=1, source_target_pairs={{0,4},{4,0},{1,5},{5,1},{2,6},{6,2},{3,7},{7,3},{8,12},{12,8},{9,1... | collective-permute-start | bytes 5505032 | tf_op jit(solution)/shard_map/ppermute | solution.py:484
  106.2 33.6 %all-to-all-start.3 = ((bf16[128,4,128]{2,1,0:T(4,128)(2,1)}), bf16[128,4,128]{2,1,0:T(4,128)(2,1)S(1)}, u32[]{:S(2)}, u32[]{:S(2)}) async-start(bf16[128,4,128]{2,1,0:T(4,128)(2,1)} %get-tuple-element.20), calls=%async_computation.3 | async-start | bytes 262144 | tf_op jit(solution)/shard_map/all_to_all | solution.py:482
  142.3 103.6 %all-to-all-start.4 = ((bf16[128,2,128]{2,1,0:T(2,128)(2,1)}), bf16[128,2,128]{2,1,0:T(2,128)(2,1)S(1)}, u32[]{:S(2)}, u32[]{:S(2)}) async-start(bf16[128,2,128]{2,1,0:T(2,128)(2,1)} %chained.1), calls=%async_computation.4 | async-start | bytes 131072 | tf_op jit(solution)/shard_map/all_to_all | solution.py:492
  166.2 83.2 %copy-start.10 = (f32[64]{0:T(128)S(1)}, f32[64]{0:T(128)}, u32[]{:S(2)}) copy-start(f32[64]{0:T(128)} %param.26) | copy-start | bytes 772
  245.9 11.4 %copy-start.5 = (bf16[128,2,128]{2,1,0:T(2,128)(2,1)}, bf16[128,2,128]{2,1,0:T(2,128)(2,1)S(1)}, u32[]{:S(2)}) copy-start(bf16[128,2,128]{2,1,0:T(2,128)(2,1)S(1)} %all-to-all-done.4) | copy-start | bytes 196612
  245.9 11.3 %all-to-all-start.2 = ((bf16[4,80,768]{2,1,0:T(8,128)(2,1)}), bf16[4,80,768]{2,1,0:T(8,128)(2,1)S(1)}, u32[]{:S(2)}, u32[]{:S(2)}) async-start(bf16[4,80,768]{2,1,0:T(8,128)(2,1)} %attention.1), calls=%async_computation.2 | async-start | bytes 983040 | tf_op jit(solution)/shard_map/all_to_all | solution.py:497
  257.3 0.8 copy-start.2
  (2 other events, 1.4 us)
where the time goes:
time: 277 us; the launch traced here: 276 us
  Pallas kernels  95.1 us (34%)
  starting transfers between devices  72.5 us (26%)
  waiting for transfers between devices  54.9 us (20%)
  blocking collectives  41.9 us (15%)
  other arithmetic  5.8 us (2%)
  local copies, waits for them, and re-layouts  5.21 us (2%)
    pallas_call x1, Pallas kernels, attention(): pl.pallas_call(attention_kernel, grid=(1,), out_shape=jax.ShapeDtypeStruc...  79.7 us
    all_to_all x2, starting transfers between devices, sent_to_all(): lax.all_to_all(jnp.broadcast_to(x[None], (size, *x.shape)), axis, 0, 0, t...  21.2 us
    ppermute x6, starting transfers between devices, from_others(): lax.ppermute(x, axis, [((k + ahead) % size, k) for k in range(size)])  19.7 us
    all_to_all x1, starting transfers between devices, body(): arrived = lax.all_to_all(sent, SP, 0, 0, tiled=True)  17.3 us
    all_to_all x1, waiting for transfers between devices, body(): arrived = lax.all_to_all(sent, SP, 0, 0, tiled=True)  15.5 us
    ppermute x6, waiting for transfers between devices, from_others(): lax.ppermute(x, axis, [((k + ahead) % size, k) for k in range(size)])  15 us
    all_gather x1, blocking collectives, body(): normed = lax.all_gather(own_normed, 'tp', axis=0, tiled=True)  14.6 us
    all_gather x1, blocking collectives, body(): all_queries = lax.all_gather(queries, 'tp', axis=0)  14.4 us
  transfers between devices with their start and end apart: 13, of which 9 were waited for; matrix products, arithmetic and copies ran while one was open for 2% of the time, Pallas kernels for 33%

commit v1 on v0

--- a/solution.py
+++ b/solution.py
@@ -370,9 +370,7 @@
     out_ref,
     ordered,
 ):
-    n_lanes = ordered.shape[1]
-    first = own_ref.shape[3] - n_lanes
-    ordered_rows(place_ref, own_ref, other_ref, slice(first, first + n_lanes), ordered)
+    ordered_rows(place_ref, own_ref, other_ref, slice(0, ordered.shape[1]), ordered)
     members = parts_ref.shape[0]
     tokens = local_ref.shape[1]
     columns = parts_ref.shape[2]
@@ -412,22 +410,23 @@
 
 def output_partial(place, second, parts, attn_gain, local, lifted, state, rec_gain, own, other):
     heads, tokens, width = local.shape
-    n_x, n_z, rows, _ = own.shape
+    n_x, n_z, rows, lanes = own.shape
     model = n_x * n_z * rows * 2
     mixed = parts.shape[2] // (2 * tokens) * HEAD_DIM + heads * width
-    arrays = (parts, attn_gain, local, lifted, state, rec_gain, own, other)
+    arrays = (parts, attn_gain, local, lifted, state, rec_gain)
+    last = pl.BlockSpec((n_x, n_z, rows, mixed), lambda *_: (0, 0, 0, lanes // mixed - 1))
     return pl.pallas_call(
         output_kernel,
         grid=(1,),
         out_shape=jax.ShapeDtypeStruct((tokens, model), jnp.bfloat16),
-        in_specs=[in_smem(), in_smem()] + [whole(a.shape) for a in arrays],
+        in_specs=[in_smem(), in_smem()] + [whole(a.shape) for a in arrays] + [last, last],
         out_specs=whole((tokens, model)),
         scratch_shapes=[pltpu.VMEM((model, mixed), jnp.bfloat16)],
         cost_estimate=pl.CostEstimate(
             flops=2 * tokens * model * mixed, bytes_accessed=2 * model * mixed, transcendentals=0
         ),
         name="output_partial",
-    )(place, second, *arrays)
+    )(place, second, *arrays, own, other)
 
 
 def body(
@@ -451,20 +450,21 @@
     place = jnp.stack([lax.axis_index("c"), lax.axis_index("x")]).astype(jnp.int32)
     own_normed = rms_scale(tokens.astype(jnp.float32), input_norm_gain).astype(jnp.bfloat16)
     own_rows = own_normed.shape[0]
-    first_payload = jnp.concatenate(
-        [recurrent_query_weight, forget_gate_weight, recurrent_value_weight], axis=1
-    )
     key_value = project(
         own_normed, jnp.concatenate([shared_key_weight, shared_value_weight], axis=1)
     )
     rows = paired_query_weight.shape[0]
     narrow = paired_query_weight.shape[1]
     kv_pieces = own_rows // rows
+    first_payload = jnp.concatenate(
+        [paired_query_weight]
+        + [key_value[k * rows : (k + 1) * rows] for k in range(kv_pieces)],
+        axis=1,
+    )
+    recurrence_weights = (recurrent_query_weight, forget_gate_weight, recurrent_value_weight)
+    recur = sum(weight.shape[1] for weight in recurrence_weights)
     second_payload = jnp.concatenate(
-        [paired_query_weight]
-        + [key_value[k * rows : (k + 1) * rows] for k in range(kv_pieces)]
-        + [attention_output_weight, recurrent_output_weight],
-        axis=1,
+        [*recurrence_weights, attention_output_weight, recurrent_output_weight], axis=1
     )
     swap = [(0, 1), (1, 0)]
     first_z = sent_to_all(first_payload, "z")
@@ -473,15 +473,18 @@
     second_z = sent_to_all(second_payload, "z")
     first_own = from_others(first_z, "x")
     first_other = lax.ppermute(first_own, "c", swap)
-    recur = first_payload.shape[1]
-    recur_raw = projections(place, first_own, first_other, normed, recur)
+    queries = projections(place, first_own, first_other, normed, narrow)
+    all_queries = lax.all_gather(queries, "tp", axis=0)
+    all_queries, second_z = lax.optimization_barrier((all_queries, second_z))
+    second_own = from_others(second_z, "x")
+    parts = attention(all_queries, (first_own, first_other), narrow // 128, kv_pieces)
+    landed_parts = lax.all_to_all(parts, "tp", 0, 0, tiled=True)
+    second_other = lax.ppermute(second_own, "c", swap)
+    recur_raw = projections(place, second_own, second_other, normed, recur)
     local_output, lifted, sent = local_recurrence(
         recur_raw, forget_leak_rate[None, :], extra_log_decay, lax.axis_size(SP)
     )
-    sent, second_z = lax.optimization_barrier((sent, second_z))
     arrived = lax.all_to_all(sent, SP, 0, 0, tiled=True)
-    second_own = from_others(second_z, "x")
-    second_other = lax.ppermute(second_own, "c", swap)
     first = lax.dynamic_index_in_dim(
         initial_recurrent_state.transpose(0, 2, 1).reshape(sent.shape[0], 2, 128),
         lax.axis_index(SP),
@@ -491,10 +494,6 @@
     before = chained(first, arrived)
     incoming_state = lax.all_to_all(before, SP, 0, 0, tiled=True)
     incoming_state = incoming_state.reshape(initial_recurrent_state.shape)
-    queries = projections(place, second_own, second_other, normed, narrow)
-    all_queries = lax.all_gather(queries, "tp", axis=0)
-    parts = attention(all_queries, (second_own, second_other), narrow // 128, kv_pieces)
-    landed_parts = lax.all_to_all(parts, "tp", 0, 0, tiled=True)
     partial = output_partial(
         place,
         second_map_weight,

time: 277 us -> 294 us (1.061)
  the two profiles are of different devices: /device:TPU:2 before, /device:TPU:1 now
where the time goes in v1:
time: 294 us; the launch traced here: 293 us
  Pallas kernels  94.5 us (32%)
  starting transfers between devices  91.9 us (31%)
  waiting for transfers between devices  55.9 us (19%)
  blocking collectives  39.8 us (14%)
  other arithmetic  4.84 us (2%)
  local copies, waits for them, and re-layouts  4.63 us (2%)
    pallas_call x1, Pallas kernels, attention(): pl.pallas_call(attention_kernel, grid=(1,), out_shape=jax.ShapeDtypeStruc...  79.7 us
    ppermute x6, waiting for transfers between devices, from_others(): lax.ppermute(x, axis, [((k + ahead) % size, k) for k in range(size)])  30 us
    all_to_all x2, starting transfers between devices, sent_to_all(): lax.all_to_all(jnp.broadcast_to(x[None], (size, *x.shape)), axis, 0, 0, t...  27 us
    ppermute x6, starting transfers between devices, from_others(): lax.ppermute(x, axis, [((k + ahead) % size, k) for k in range(size)])  20.1 us
    all_to_all x1, starting transfers between devices, body(): incoming_state = lax.all_to_all(before, SP, 0, 0, tiled=True)  17.8 us
    all_to_all x1, starting transfers between devices, body(): arrived = lax.all_to_all(sent, SP, 0, 0, tiled=True)  15.4 us
    all_to_all x1, blocking collectives, body(): landed = lax.all_to_all(blocks, 'tp', 0, 0, tiled=True)  15.3 us
    all_to_all x1, waiting for transfers between devices, body(): incoming_state = lax.all_to_all(before, SP, 0, 0, tiled=True)  14.2 us
  transfers between devices with their start and end apart: 13, of which 10 were waited for; matrix products, arithmetic and copies ran while one was open for 1% of the time, Pallas kernels for 29%

profile of v1, /device:TPU:1, one launch (start us, length us, event | category | flops | bytes accessed | tf_op | source)
XLA Modules:
  0.0 293.2 jit_solution(2972932020934630410)
XLA Ops:
  5.0 15.7 %all-to-all-start = ((bf16[16,16,512]{2,1,0:T(8,128)(2,1)}), bf16[16,16,512]{2,1,0:T(8,128)(2,1)S(1)}, u32[]{:S(2)}, u32[]{:S(2)}) async-start(bf16[16,16,512]{2,1,0:T(8,128)(2,1)} %broadcast_in_dim.10), calls=%async_computation | async-start | bytes 524288 | tf_op jit(solution)/shard_map/all_to_all | solution.py:28
  20.8 13.2 %all_gather.9.normed_ref = bf16[192,2048]{1,0:T(8,128)(2,1)} all-gather(bf16[48,2048]{1,0:T(8,128)(2,1)S(1)} %fusion.5), channel_id=1, replica_groups=mesh['z'=16,'x'=4,'c'=2,'tp'=4] {'tp'}, dimensions={0}, use_global_device_ids=true | all-gather | bytes 983040 | tf_op jit(solution)/shard_map/all_gather | solution.py:471
  35.4 11.2 %all-to-all-start.1 = ((bf16[16,16,1152]{2,1,0:T(8,128)(2,1)}), bf16[16,16,1152]{2,1,0:T(8,128)(2,1)S(1)}, u32[]{:S(2)}, u32[]{:S(2)}) async-start(bf16[16,16,1152]{2,1,0:T(8,128)(2,1)} %broadcast_in_dim.11), calls=%async_computation.1 | async-start | bytes 1179648 | tf_op jit(solution)/shard_map/all_to_all | solution.py:28
  46.6 3.1 %collective-permute-start.2 = (bf16[16,16,512]{2,1,0:T(8,128)(2,1)S(1)}, bf16[16,16,512]{2,1,0:T(8,128)(2,1)S(1)}, u32[]{:S(2)}, u32[]{:S(2)}) collective-permute-start(bf16[16,16,512]{2,1,0:T(8,128)(2,1)S(1)} %all-to-all-done), channel_id=1, source_target_pairs={{24,0},{0,8},{8,16},{16,24},{25,1},{1,9},{9,17},{17,25},{26,2},{2,... | collective-permute-start | bytes 786440 | tf_op jit(solution)/shard_map/ppermute | solution.py:34
  49.7 4.4 %collective-permute-start.1 = (bf16[16,16,512]{2,1,0:T(8,128)(2,1)S(1)}, bf16[16,16,512]{2,1,0:T(8,128)(2,1)S(1)}, u32[]{:S(2)}, u32[]{:S(2)}) collective-permute-start(bf16[16,16,512]{2,1,0:T(8,128)(2,1)S(1)} %all-to-all-done), channel_id=1, source_target_pairs={{16,0},{24,8},{0,16},{8,24},{17,1},{25,9},{1,17},{9,25},{18,2},{26... | collective-permute-start | bytes 786440 | tf_op jit(solution)/shard_map/ppermute | solution.py:34
  54.1 3.1 %collective-permute-start = (bf16[16,16,512]{2,1,0:T(8,128)(2,1)S(1)}, bf16[16,16,512]{2,1,0:T(8,128)(2,1)S(1)}, u32[]{:S(2)}, u32[]{:S(2)}) collective-permute-start(bf16[16,16,512]{2,1,0:T(8,128)(2,1)S(1)} %all-to-all-done), channel_id=1, source_target_pairs={{8,0},{16,8},{24,16},{0,24},{9,1},{17,9},{25,17},{1,25},{10,2},{18... | collective-permute-start | bytes 786440 | tf_op jit(solution)/shard_map/ppermute | solution.py:34
  57.2 4.3 %collective-permute-done.1 = bf16[16,16,512]{2,1,0:T(8,128)(2,1)S(1)} collective-permute-done((bf16[16,16,512]{2,1,0:T(8,128)(2,1)S(1)}, bf16[16,16,512]{2,1,0:T(8,128)(2,1)S(1)}, u32[]{:S(2)}, u32[]{:S(2)}) %collective-permute-start.1) | collective-permute-done | bytes 262176 | tf_op jit(solution)/shard_map/ppermute | solution.py:34
  64.5 4.7 %collective-permute-start.3 = (bf16[4,16,16,512]{3,2,1,0:T(8,128)(2,1)S(1)}, bf16[4,16,16,512]{3,2,1,0:T(8,128)(2,1)S(1)}, u32[]{:S(2)}, u32[]{:S(2)}) collective-permute-start(bf16[4,16,16,512]{3,2,1,0:T(8,128)(2,1)S(1)} %pad_maximum_fusion.1.own_ref.refs_0_.refs_1_.refs_2_), channel_id=1, source_target_pairs={{0,4},{4,0},{1,5},{5,1},{2,6},{6,2},{3,7},{7,3},{8,12},{12,8},{9,1... | collective-permute-start | bytes 3145736 | tf_op jit(solution)/shard_map/ppermute | solution.py:475
  74.9 11.2 %all-gather = bf16[768,128]{1,0:T(8,128)(2,1)} all-gather(bf16[192,128]{1,0:T(8,128)(2,1)} %shard_map.154), channel_id=2, replica_groups=mesh['z'=16,'x'=4,'c'=2,'tp'=4] {'tp'}, dimensions={0}, use_global_device_ids=true | all-gather | bytes 245760 | tf_op jit(solution)/shard_map/all_gather | solution.py:477
  89.2 4.3 %collective-permute-start.5 = (bf16[16,16,1152]{2,1,0:T(8,128)(2,1)S(1)}, bf16[16,16,1152]{2,1,0:T(8,128)(2,1)S(1)}, u32[]{:S(2)}, u32[]{:S(2)}) collective-permute-start(bf16[16,16,1152]{2,1,0:T(8,128)(2,1)S(1)} %all-to-all-done.1), channel_id=1, source_target_pairs={{16,0},{24,8},{0,16},{8,24},{17,1},{25,9},{1,17},{9,25},{18,2},{26... | collective-permute-start | bytes 1769480 | tf_op jit(solution)/shard_map/ppermute | solution.py:34
  95.8 5.4 %collective-permute-done.6 = bf16[16,16,1152]{2,1,0:T(8,128)(2,1)S(1)} collective-permute-done((bf16[16,16,1152]{2,1,0:T(8,128)(2,1)S(1)}, bf16[16,16,1152]{2,1,0:T(8,128)(2,1)S(1)}, u32[]{:S(2)}, u32[]{:S(2)}) %collective-permute-start.6) | collective-permute-done | bytes 589856 | tf_op jit(solution)/shard_map/ppermute | solution.py:34
  101.1 13.5 %collective-permute-done.5 = bf16[16,16,1152]{2,1,0:T(8,128)(2,1)S(1)} collective-permute-done((bf16[16,16,1152]{2,1,0:T(8,128)(2,1)S(1)}, bf16[16,16,1152]{2,1,0:T(8,128)(2,1)S(1)}, u32[]{:S(2)}, u32[]{:S(2)}) %collective-permute-start.5) | collective-permute-done | bytes 589856 | tf_op jit(solution)/shard_map/ppermute | solution.py:34
  114.7 3.9 %collective-permute-done.4 = bf16[16,16,1152]{2,1,0:T(8,128)(2,1)S(1)} collective-permute-done((bf16[16,16,1152]{2,1,0:T(8,128)(2,1)S(1)}, bf16[16,16,1152]{2,1,0:T(8,128)(2,1)S(1)}, u32[]{:S(2)}, u32[]{:S(2)}) %collective-permute-start.4) | collective-permute-done | bytes 589856 | tf_op jit(solution)/shard_map/ppermute | solution.py:34
  119.0 3.5 %collective-permute-start.7 = (bf16[4,16,16,1152]{3,2,1,0:T(8,128)(2,1)S(1)}, bf16[4,16,16,1152]{3,2,1,0:T(8,128)(2,1)}, u32[]{:S(2)}, u32[]{:S(2)}) collective-permute-start(bf16[4,16,16,1152]{3,2,1,0:T(8,128)(2,1)S(1)} %pad_maximum_fusion.own_ref), channel_id=1, source_target_pairs={{0,4},{4,0},{1,5},{5,1},{2,6},{6,2},{3,7},{7,3},{8,12},{12,8},{9,1... | collective-permute-start | bytes 7077896 | tf_op jit(solution)/shard_map/ppermute | solution.py:482
  122.4 4.3 %collective-permute-done.7.other_ref = bf16[4,16,16,1152]{3,2,1,0:T(8,128)(2,1)} collective-permute-done((bf16[4,16,16,1152]{3,2,1,0:T(8,128)(2,1)S(1)}, bf16[4,16,16,1152]{3,2,1,0:T(8,128)(2,1)}, u32[]{:S(2)}, u32[]{:S(2)}) %collective-permute-start.7) | collective-permute-done | bytes 2359328 | tf_op jit(solution)/shard_map/ppermute | solution.py:482
  126.7 3.8 %shard_map.155.raw_ref = bf16[192,768]{1,0:T(8,128)(2,1)} custom-call(s32[2]{0:T(128)} %pad_add_fusion.place_ref, bf16[4,16,16,1152]{3,2,1,0:T(8,128)(2,1)} %copy-done, bf16[4,16,16,1152]{3,2,1,0:T(8,128)(2,1)} %collective-permute-done.7.other_ref, bf16[192,2048]{1,0:T(8,128)(2,1)} %all_gather.9.normed_ref), custom_call_target="tpu_custom_call" | custom-call | flops 603979776 | bytes 3145728 | tf_op jit(solution)/shard_map/pallas_call | solution.py:90
  133.5 15.4 %all-to-all-start.3 = ((bf16[128,4,128]{2,1,0:T(4,128)(2,1)}), bf16[128,4,128]{2,1,0:T(4,128)(2,1)S(1)}, u32[]{:S(2)}, u32[]{:S(2)}) async-start(bf16[128,4,128]{2,1,0:T(4,128)(2,1)} %get-tuple-element.20), calls=%async_computation.3 | async-start | bytes 262144 | tf_op jit(solution)/shard_map/all_to_all | solution.py:487
  148.9 79.7 %attention.1 = bf16[4,80,768]{2,1,0:T(8,128)(2,1)} custom-call(bf16[4,192,128]{2,1,0:T(8,128)(2,1)} %bitcast.32, bf16[4,16,16,512]{3,2,1,0:T(8,128)(2,1)} %copy-done.1, bf16[4,16,16,512]{3,2,1,0:T(8,128)(2,1)} %copy-done.1, bf16[4,16,16,512]{3,2,1,0:T(8,128)(2,1)} %copy-done.1, bf16[4,16,16,512]{3,2,1,0:T(8,128)(2,1)} %copy-done.3, ...), custom_call_target="tpu_custom_call" | custom-call | flops 19327352832 | bytes 1572864 | tf_op jit(solution)/shard_map/attention/pallas_call | solution.py:238
  228.6 3.5 %all-to-all-start.2 = ((bf16[4,80,768]{2,1,0:T(8,128)(2,1)}), bf16[4,80,768]{2,1,0:T(8,128)(2,1)S(1)}, u32[]{:S(2)}, u32[]{:S(2)}) async-start(bf16[4,80,768]{2,1,0:T(8,128)(2,1)} %attention.1), calls=%async_computation.2 | async-start | bytes 983040 | tf_op jit(solution)/shard_map/all_to_all | solution.py:481
  234.7 5.5 %all-to-all-done.2.parts_ref = bf16[4,80,768]{2,1,0:T(8,128)(2,1)S(1)} async-done(((bf16[4,80,768]{2,1,0:T(8,128)(2,1)}), bf16[4,80,768]{2,1,0:T(8,128)(2,1)S(1)}, u32[]{:S(2)}, u32[]{:S(2)}) %all-to-all-start.2) | async-done | bytes 491552 | tf_op jit(solution)/shard_map/all_to_all | solution.py:481
  240.1 17.8 %all-to-all-start.4 = ((bf16[128,2,128]{2,1,0:T(2,128)(2,1)}), bf16[128,2,128]{2,1,0:T(2,128)(2,1)S(1)}, u32[]{:S(2)}, u32[]{:S(2)}) async-start(bf16[128,2,128]{2,1,0:T(2,128)(2,1)} %chained.1), calls=%async_computation.4 | async-start | bytes 131072 | tf_op jit(solution)/shard_map/all_to_all | solution.py:495
  258.6 14.2 %all-to-all-done.4 = bf16[128,2,128]{2,1,0:T(2,128)(2,1)S(1)} async-done(((bf16[128,2,128]{2,1,0:T(2,128)(2,1)}), bf16[128,2,128]{2,1,0:T(2,128)(2,1)S(1)}, u32[]{:S(2)}, u32[]{:S(2)}) %all-to-all-start.4) | async-done | bytes 65568 | tf_op jit(solution)/shard_map/all_to_all | solution.py:495
  273.4 3.7 %output_partial.1 = bf16[192,2048]{1,0:T(8,128)(2,1)} custom-call(s32[2]{0:T(128)} %pad_add_fusion.place_ref, f32[2]{0:T(128)} %second_ref.1, bf16[4,80,768]{2,1,0:T(8,128)(2,1)} %copy-done.2, f32[64,1]{1,0:T(8,128)} %copy.19.attn_gain_ref, f32[2,192,128]{2,1,0:T(8,128)} %get-tuple-element.18.local_ref, bf16[2,192,128]{2,1,0:T(8,128)(2,1)} %get-tuple-element.19.lifted_ref, ...), custom_call_target="tpu_custom_call" | custom-call | flops 301989888 | bytes 1572864 | tf_op jit(solution)/shard_map/output_partial/pallas_call | solution.py:418
  277.0 15.3 %all_to_all.30 = bf16[4,48,2048]{2,1,0:T(8,128)(2,1)S(1)} all-to-all(bf16[4,48,2048]{2,1,0:T(8,128)(2,1)} %bitcast.22), channel_id=1, replica_groups=mesh['z'=16,'x'=4,'c'=2,'tp'=4] {'tp'}, dimensions={0} | all-to-all | bytes 1572864 | tf_op jit(solution)/shard_map/all_to_all | solution.py:511
  (57 shorter events, 28.2 us)
Async XLA Ops:
  0.0 20.7 %copy-start.7 = (bf16[16,256]{1,0:T(8,128)(2,1)S(1)}, bf16[16,256]{1,0:T(8,128)(2,1)}, u32[]{:S(2)}) copy-start(bf16[16,256]{1,0:T(8,128)(2,1)} %param.21) | copy-start | bytes 24580
  0.0 20.7 %copy-start.8 = (bf16[16,256]{1,0:T(8,128)(2,1)S(1)}, bf16[16,256]{1,0:T(8,128)(2,1)}, u32[]{:S(2)}) copy-start(bf16[16,256]{1,0:T(8,128)(2,1)} %param.22) | copy-start | bytes 24580
  0.0 20.8 %copy-start.9 = (bf16[16,256]{1,0:T(8,128)(2,1)S(1)}, bf16[16,256]{1,0:T(8,128)(2,1)}, u32[]{:S(2)}) copy-start(bf16[16,256]{1,0:T(8,128)(2,1)} %param.23) | copy-start | bytes 24580
  0.0 20.8 %copy-start.11 = (bf16[16,128]{1,0:T(8,128)(2,1)S(1)}, bf16[16,128]{1,0:T(8,128)(2,1)}, u32[]{:S(2)}) copy-start(bf16[16,128]{1,0:T(8,128)(2,1)} %param.24) | copy-start | bytes 12292
  0.0 20.8 %copy-start.10 = (bf16[16,256]{1,0:T(8,128)(2,1)S(1)}, bf16[16,256]{1,0:T(8,128)(2,1)}, u32[]{:S(2)}) copy-start(bf16[16,256]{1,0:T(8,128)(2,1)} %param.25) | copy-start | bytes 24580
  5.0 29.5 %all-to-all-start = ((bf16[16,16,512]{2,1,0:T(8,128)(2,1)}), bf16[16,16,512]{2,1,0:T(8,128)(2,1)S(1)}, u32[]{:S(2)}, u32[]{:S(2)}) async-start(bf16[16,16,512]{2,1,0:T(8,128)(2,1)} %broadcast_in_dim.10), calls=%async_computation | async-start | bytes 524288 | tf_op jit(solution)/shard_map/all_to_all | solution.py:28
  35.4 50.8 %all-to-all-start.1 = ((bf16[16,16,1152]{2,1,0:T(8,128)(2,1)}), bf16[16,16,1152]{2,1,0:T(8,128)(2,1)S(1)}, u32[]{:S(2)}, u32[]{:S(2)}) async-start(bf16[16,16,1152]{2,1,0:T(8,128)(2,1)} %broadcast_in_dim.11), calls=%async_computation.1 | async-start | bytes 1179648 | tf_op jit(solution)/shard_map/all_to_all | solution.py:28
  46.6 10.6 %collective-permute-start.2 = (bf16[16,16,512]{2,1,0:T(8,128)(2,1)S(1)}, bf16[16,16,512]{2,1,0:T(8,128)(2,1)S(1)}, u32[]{:S(2)}, u32[]{:S(2)}) collective-permute-start(bf16[16,16,512]{2,1,0:T(8,128)(2,1)S(1)} %all-to-all-done), channel_id=1, source_target_pairs={{24,0},{0,8},{8,16},{16,24},{25,1},{1,9},{9,17},{17,25},{26,2},{2,... | collective-permute-start | bytes 786440 | tf_op jit(solution)/shard_map/ppermute | solution.py:34
  49.7 11.8 %collective-permute-start.1 = (bf16[16,16,512]{2,1,0:T(8,128)(2,1)S(1)}, bf16[16,16,512]{2,1,0:T(8,128)(2,1)S(1)}, u32[]{:S(2)}, u32[]{:S(2)}) collective-permute-start(bf16[16,16,512]{2,1,0:T(8,128)(2,1)S(1)} %all-to-all-done), channel_id=1, source_target_pairs={{16,0},{24,8},{0,16},{8,24},{17,1},{25,9},{1,17},{9,25},{18,2},{26... | collective-permute-start | bytes 786440 | tf_op jit(solution)/shard_map/ppermute | solution.py:34
  54.1 10.2 %collective-permute-start = (bf16[16,16,512]{2,1,0:T(8,128)(2,1)S(1)}, bf16[16,16,512]{2,1,0:T(8,128)(2,1)S(1)}, u32[]{:S(2)}, u32[]{:S(2)}) collective-permute-start(bf16[16,16,512]{2,1,0:T(8,128)(2,1)S(1)} %all-to-all-done), channel_id=1, source_target_pairs={{8,0},{16,8},{24,16},{0,24},{9,1},{17,9},{25,17},{1,25},{10,2},{18... | collective-permute-start | bytes 786440 | tf_op jit(solution)/shard_map/ppermute | solution.py:34
  64.5 7.0 %copy-start.1 = (bf16[4,16,16,512]{3,2,1,0:T(8,128)(2,1)}, bf16[4,16,16,512]{3,2,1,0:T(8,128)(2,1)S(1)}, u32[]{:S(2)}) copy-start(bf16[4,16,16,512]{3,2,1,0:T(8,128)(2,1)S(1)} %pad_maximum_fusion.1.own_ref.refs_0_.refs_1_.refs_2_) | copy-start | bytes 3145732
  64.5 7.0 %collective-permute-start.3 = (bf16[4,16,16,512]{3,2,1,0:T(8,128)(2,1)S(1)}, bf16[4,16,16,512]{3,2,1,0:T(8,128)(2,1)S(1)}, u32[]{:S(2)}, u32[]{:S(2)}) collective-permute-start(bf16[4,16,16,512]{3,2,1,0:T(8,128)(2,1)S(1)} %pad_maximum_fusion.1.own_ref.refs_0_.refs_1_.refs_2_), channel_id=1, source_target_pairs={{0,4},{4,0},{1,5},{5,1},{2,6},{6,2},{3,7},{7,3},{8,12},{12,8},{9,1... | collective-permute-start | bytes 3145736 | tf_op jit(solution)/shard_map/ppermute | solution.py:475
  86.1 15.0 %collective-permute-start.6 = (bf16[16,16,1152]{2,1,0:T(8,128)(2,1)S(1)}, bf16[16,16,1152]{2,1,0:T(8,128)(2,1)S(1)}, u32[]{:S(2)}, u32[]{:S(2)}) collective-permute-start(bf16[16,16,1152]{2,1,0:T(8,128)(2,1)S(1)} %all-to-all-done.1), channel_id=1, source_target_pairs={{24,0},{0,8},{8,16},{16,24},{25,1},{1,9},{9,17},{17,25},{26,2},{2,... | collective-permute-start | bytes 1769480 | tf_op jit(solution)/shard_map/ppermute | solution.py:34
  89.2 25.5 %collective-permute-start.5 = (bf16[16,16,1152]{2,1,0:T(8,128)(2,1)S(1)}, bf16[16,16,1152]{2,1,0:T(8,128)(2,1)S(1)}, u32[]{:S(2)}, u32[]{:S(2)}) collective-permute-start(bf16[16,16,1152]{2,1,0:T(8,128)(2,1)S(1)} %all-to-all-done.1), channel_id=1, source_target_pairs={{16,0},{24,8},{0,16},{8,24},{17,1},{25,9},{1,17},{9,25},{18,2},{26... | collective-permute-start | bytes 1769480 | tf_op jit(solution)/shard_map/ppermute | solution.py:34
  93.5 25.1 %collective-permute-start.4 = (bf16[16,16,1152]{2,1,0:T(8,128)(2,1)S(1)}, bf16[16,16,1152]{2,1,0:T(8,128)(2,1)S(1)}, u32[]{:S(2)}, u32[]{:S(2)}) collective-permute-start(bf16[16,16,1152]{2,1,0:T(8,128)(2,1)S(1)} %all-to-all-done.1), channel_id=1, source_target_pairs={{8,0},{16,8},{24,16},{0,24},{9,1},{17,9},{25,17},{1,25},{10,2},{18... | collective-permute-start | bytes 1769480 | tf_op jit(solution)/shard_map/ppermute | solution.py:34
  119.0 7.8 %copy-start = (bf16[4,16,16,1152]{3,2,1,0:T(8,128)(2,1)}, bf16[4,16,16,1152]{3,2,1,0:T(8,128)(2,1)S(1)}, u32[]{:S(2)}) copy-start(bf16[4,16,16,1152]{3,2,1,0:T(8,128)(2,1)S(1)} %pad_maximum_fusion.own_ref) | copy-start | bytes 7077892
  119.0 7.7 %collective-permute-start.7 = (bf16[4,16,16,1152]{3,2,1,0:T(8,128)(2,1)S(1)}, bf16[4,16,16,1152]{3,2,1,0:T(8,128)(2,1)}, u32[]{:S(2)}, u32[]{:S(2)}) collective-permute-start(bf16[4,16,16,1152]{3,2,1,0:T(8,128)(2,1)S(1)} %pad_maximum_fusion.own_ref), channel_id=1, source_target_pairs={{0,4},{4,0},{1,5},{5,1},{2,6},{6,2},{3,7},{7,3},{8,12},{12,8},{9,1... | collective-permute-start | bytes 7077896 | tf_op jit(solution)/shard_map/ppermute | solution.py:482
  133.5 95.2 %all-to-all-start.3 = ((bf16[128,4,128]{2,1,0:T(4,128)(2,1)}), bf16[128,4,128]{2,1,0:T(4,128)(2,1)S(1)}, u32[]{:S(2)}, u32[]{:S(2)}) async-start(bf16[128,4,128]{2,1,0:T(4,128)(2,1)} %get-tuple-element.20), calls=%async_computation.3 | async-start | bytes 262144 | tf_op jit(solution)/shard_map/all_to_all | solution.py:487
  148.9 83.3 %copy-start.6 = (f32[2,128,128]{2,1,0:T(8,128)S(1)}, f32[2,128,128]{2,1,0:T(8,128)}, u32[]{:S(2)}) copy-start(f32[2,128,128]{2,1,0:T(8,128)} %param.31) | copy-start | bytes 393220
  148.9 109.0 %copy-start.12 = (f32[64]{0:T(128)S(1)}, f32[64]{0:T(128)}, u32[]{:S(2)}) copy-start(f32[64]{0:T(128)} %param.26) | copy-start | bytes 772
  228.6 4.2 %copy-start.4 = (bf16[128,4,128]{2,1,0:T(4,128)(2,1)}, bf16[128,4,128]{2,1,0:T(4,128)(2,1)S(1)}, u32[]{:S(2)}) copy-start(bf16[128,4,128]{2,1,0:T(4,128)(2,1)S(1)} %all-to-all-done.3.pieces_ref) | copy-start | bytes 393220
  228.6 11.5 %all-to-all-start.2 = ((bf16[4,80,768]{2,1,0:T(8,128)(2,1)}), bf16[4,80,768]{2,1,0:T(8,128)(2,1)S(1)}, u32[]{:S(2)}, u32[]{:S(2)}) async-start(bf16[4,80,768]{2,1,0:T(8,128)(2,1)} %attention.1), calls=%async_computation.2 | async-start | bytes 983040 | tf_op jit(solution)/shard_map/all_to_all | solution.py:481
  240.1 32.6 %copy-start.2 = (bf16[4,80,768]{2,1,0:T(8,128)(2,1)}, bf16[4,80,768]{2,1,0:T(8,128)(2,1)S(1)}, u32[]{:S(2)}) copy-start(bf16[4,80,768]{2,1,0:T(8,128)(2,1)S(1)} %all-to-all-done.2.parts_ref) | copy-start | bytes 1474564
  240.1 32.6 %all-to-all-start.4 = ((bf16[128,2,128]{2,1,0:T(2,128)(2,1)}), bf16[128,2,128]{2,1,0:T(2,128)(2,1)S(1)}, u32[]{:S(2)}, u32[]{:S(2)}) async-start(bf16[128,2,128]{2,1,0:T(2,128)(2,1)} %chained.1), calls=%async_computation.4 | async-start | bytes 131072 | tf_op jit(solution)/shard_map/all_to_all | solution.py:495
  (2 other events, 1.6 us)

commit v2 on v1

--- a/solution.py
+++ b/solution.py
@@ -15,10 +15,12 @@
 RECURRENT_WIDTH = 128
 REC_SPAN = 64
 SP = ("z", "x", "c")
+PLANE = ("x", "c")
 SP_TP = ("z", "x", "c", "tp")
 KEY_BLOCK = 512
 COLUMN_TILE = 256
 PART_ROWS = 80
+DECAY_ROWS = 16
 
 epsilon = 1e-06
 
@@ -57,11 +59,11 @@
     return jnp.dot(a, b, preferred_element_type=jnp.float32)
 
 
-def ordered_rows(place_ref, own_ref, other_ref, lanes, ordered):
+def ordered_rows(place_ref, own_ref, other_ref, lanes, ordered, from_own):
     n_x, n_z, rows = own_ref.shape[:3]
     core = place_ref[0]
     for x in range(n_x):
-        owner = lax.rem(place_ref[1] + x, n_x)
+        owner = lax.rem(place_ref[1] + x, n_x) if from_own else x
         for z in range(n_z):
             start = (z * n_x + owner) * 2 * rows
             mine = pl.multiple_of(start + core * rows, rows)
@@ -70,9 +72,9 @@
             ordered[pl.ds(others, rows), :] = other_ref[x, z, :, lanes]
 
 
-def projection_kernel(place_ref, own_ref, other_ref, normed_ref, out_ref, ordered):
+def projection_kernel(from_own, place_ref, own_ref, other_ref, normed_ref, out_ref, ordered):
     wide = out_ref.shape[1]
-    ordered_rows(place_ref, own_ref, other_ref, slice(0, wide), ordered)
+    ordered_rows(place_ref, own_ref, other_ref, slice(0, wide), ordered, from_own)
     normed = normed_ref[...]
     step = min(wide, 256)
     for k in range(wide // step):
@@ -84,11 +86,11 @@
     return pl.BlockSpec(memory_space=pltpu.SMEM)
 
 
-def projections(place, own, other, normed, wide):
+def projections(place, own, other, normed, wide, from_own):
     tokens, width = normed.shape
     piece = (*own.shape[:3], wide)
     return pl.pallas_call(
-        projection_kernel,
+        functools.partial(projection_kernel, from_own),
         grid=(1,),
         out_shape=jax.ShapeDtypeStruct((tokens, wide), jnp.bfloat16),
         in_specs=[in_smem(), whole(piece), whole(piece), whole(normed.shape)],
@@ -262,7 +264,7 @@
     return high, middle, (rest - middle.astype(jnp.float32)).astype(jnp.bfloat16)
 
 
-def recurrence_kernel(raw_ref, leak_ref, extra_ref, local_ref, lifted_ref, sent_ref, held):
+def recurrence_kernel(raw_ref, leak_ref, extra_ref, local_ref, lifted_ref, sent_ref):
     rows, wide = extra_ref.shape
     heads = wide // RECURRENT_WIDTH
     raw_query = raw_ref[:, :wide].astype(jnp.float32)
@@ -300,23 +302,23 @@
                 values, closing[:, lanes], (((0,), (0,)), ((), ())),
                 preferred_element_type=jnp.float32,
             )
-    held[heads * RECURRENT_WIDTH :, :] = jnp.zeros((8, RECURRENT_WIDTH), jnp.float32)
-    for head in range(heads):
-        held[head * RECURRENT_WIDTH : (head + 1) * RECURRENT_WIDTH, :] = states[head]
-    members = sent_ref.shape[0]
-    state_row = lax.broadcasted_iota(jnp.int32, (4, RECURRENT_WIDTH), 0) < 2
+    members, piece_rows, _ = sent_ref.shape
+    share = heads * RECURRENT_WIDTH // members
     decays = jnp.exp(offset)
     for k in range(members):
-        head = k * heads // members
+        head, start = k * share // RECURRENT_WIDTH, k * share % RECURRENT_WIDTH
         decay = decays[:, head * RECURRENT_WIDTH : (head + 1) * RECURRENT_WIDTH]
-        sent_ref[k] = jnp.where(state_row, held[2 * k : 2 * k + 4, :], decay).astype(jnp.bfloat16)
+        sent_ref[k, :share, :] = states[head][start : start + share].astype(jnp.bfloat16)
+        sent_ref[k, share:, :] = jnp.broadcast_to(
+            decay, (piece_rows - share, RECURRENT_WIDTH)
+        ).astype(jnp.bfloat16)
 
 
 def local_recurrence(raw, leak, extra, members):
     rows, wide = extra.shape
     heads = wide // RECURRENT_WIDTH
     by_head = (heads, rows, RECURRENT_WIDTH)
-    sent = (members, 4, RECURRENT_WIDTH)
+    sent = (members, heads * RECURRENT_WIDTH // members + DECAY_ROWS, RECURRENT_WIDTH)
     return pl.pallas_call(
         recurrence_kernel,
         grid=(1,),
@@ -327,7 +329,6 @@
         ),
         in_specs=[whole(raw.shape), whole(leak.shape), whole(extra.shape)],
         out_specs=(whole(by_head), whole(by_head), whole(sent)),
-        scratch_shapes=[pltpu.VMEM((heads * RECURRENT_WIDTH + 8, RECURRENT_WIDTH), jnp.float32)],
         cost_estimate=pl.CostEstimate(
             flops=2 * rows * wide * 1024, bytes_accessed=8 * rows * wide, transcendentals=0
         ),
@@ -335,25 +336,62 @@
     )(raw, leak, extra)
 
 
-def chain_kernel(first_ref, pieces_ref, out_ref):
-    def visit(k, state):
+def passed(pieces_ref, k, state, share):
+    decay = pieces_ref[k, share : share + 1, :].astype(jnp.float32)
+    return decay * state + pieces_ref[k, :share, :].astype(jnp.float32), decay
+
+
+def plane_kernel(pieces_ref, out_ref):
+    members, piece_rows, width = pieces_ref.shape
+    share = piece_rows - DECAY_ROWS
+    state = jnp.zeros((share, width), jnp.float32)
+    total = jnp.ones((1, width), jnp.float32)
+    for k in range(members):
+        state, decay = passed(pieces_ref, k, state, share)
+        total = total * decay
+    state = state.astype(jnp.bfloat16)
+    total = jnp.broadcast_to(total, (DECAY_ROWS, width)).astype(jnp.bfloat16)
+    for k in range(out_ref.shape[0]):
+        out_ref[k, :share, :] = state
+        out_ref[k, share:, :] = total
+
+
+def before_kernel(place_ref, first_ref, planes_ref, pieces_ref, out_ref):
+    members, share, _ = out_ref.shape
+    mine = place_ref[1] * 2 + place_ref[0]
+    state = lax.fori_loop(
+        0,
+        place_ref[2],
+        lambda k, state: passed(planes_ref, k, state, share)[0],
+        first_ref[mine],
+    )
+    for k in range(members):
         out_ref[k] = state.astype(jnp.bfloat16)
-        piece = pieces_ref[k].astype(jnp.float32)
-        return piece[2:3, :] * state + piece[0:2, :]
-
-    lax.fori_loop(0, pieces_ref.shape[0], visit, first_ref[...], unroll=8)
-
-
-def chained(first, pieces):
-    count = pieces.shape[0]
+        state, _ = passed(pieces_ref, k, state, share)
+
+
+def plane_total(pieces, planes):
+    out = (planes, *pieces.shape[1:])
     return pl.pallas_call(
-        chain_kernel,
+        plane_kernel,
         grid=(1,),
-        out_shape=jax.ShapeDtypeStruct((count, 2, 128), jnp.bfloat16),
-        in_specs=[whole(first.shape), whole(pieces.shape)],
-        out_specs=whole((count, 2, 128)),
-        name="chained",
-    )(first, pieces)
+        out_shape=jax.ShapeDtypeStruct(out, jnp.bfloat16),
+        in_specs=[whole(pieces.shape)],
+        out_specs=whole(out),
+        name="plane_total",
+    )(pieces)
+
+
+def states_before(place, first, planes, pieces):
+    arrays = (first, planes, pieces)
+    return pl.pallas_call(
+        before_kernel,
+        grid=(1,),
+        out_shape=jax.ShapeDtypeStruct(first.shape, jnp.bfloat16),
+        in_specs=[in_smem()] + [whole(a.shape) for a in arrays],
+        out_specs=whole(first.shape),
+        name="states_before",
+    )(place, *arrays)
 
 
 def output_kernel(
@@ -370,7 +408,7 @@
     out_ref,
     ordered,
 ):
-    ordered_rows(place_ref, own_ref, other_ref, slice(0, ordered.shape[1]), ordered)
+    ordered_rows(place_ref, own_ref, other_ref, slice(0, ordered.shape[1]), ordered, False)
     members = parts_ref.shape[0]
     tokens = local_ref.shape[1]
     columns = parts_ref.shape[2]
@@ -447,7 +485,7 @@
     extra_log_decay,
     initial_recurrent_state,
 ):
-    place = jnp.stack([lax.axis_index("c"), lax.axis_index("x")]).astype(jnp.int32)
+    place = jnp.stack([lax.axis_index(axis) for axis in ("c", "x", "z")]).astype(jnp.int32)
     own_normed = rms_scale(tokens.astype(jnp.float32), input_norm_gain).astype(jnp.bfloat16)
     own_rows = own_normed.shape[0]
     key_value = project(
@@ -473,26 +511,24 @@
     second_z = sent_to_all(second_payload, "z")
     first_own = from_others(first_z, "x")
     first_other = lax.ppermute(first_own, "c", swap)
-    queries = projections(place, first_own, first_other, normed, narrow)
+    queries = projections(place, first_own, first_other, normed, narrow, True)
     all_queries = lax.all_gather(queries, "tp", axis=0)
     all_queries, second_z = lax.optimization_barrier((all_queries, second_z))
-    second_own = from_others(second_z, "x")
+    second_own = sent_to_all(second_z, "x")
     parts = attention(all_queries, (first_own, first_other), narrow // 128, kv_pieces)
     landed_parts = lax.all_to_all(parts, "tp", 0, 0, tiled=True)
     second_other = lax.ppermute(second_own, "c", swap)
-    recur_raw = projections(place, second_own, second_other, normed, recur)
+    recur_raw = projections(place, second_own, second_other, normed, recur, False)
+    members = lax.axis_size(PLANE)
     local_output, lifted, sent = local_recurrence(
-        recur_raw, forget_leak_rate[None, :], extra_log_decay, lax.axis_size(SP)
-    )
-    arrived = lax.all_to_all(sent, SP, 0, 0, tiled=True)
-    first = lax.dynamic_index_in_dim(
-        initial_recurrent_state.transpose(0, 2, 1).reshape(sent.shape[0], 2, 128),
-        lax.axis_index(SP),
-        0,
-        False,
-    )
-    before = chained(first, arrived)
-    incoming_state = lax.all_to_all(before, SP, 0, 0, tiled=True)
+        recur_raw, forget_leak_rate[None, :], extra_log_decay, members
+    )
+    pieces = lax.all_to_all(sent, PLANE, 0, 0, tiled=True)
+    total = plane_total(pieces, lax.axis_size("z"))
+    planes = lax.all_to_all(total, "z", 0, 0, tiled=True)
+    first = initial_recurrent_state.transpose(0, 2, 1).reshape(members, -1, RECURRENT_WIDTH)
+    before = states_before(place, first, planes, pieces)
+    incoming_state = lax.all_to_all(before, PLANE, 0, 0, tiled=True)
     incoming_state = incoming_state.reshape(initial_recurrent_state.shape)
     partial = output_partial(
         place,

time: 294 us -> 278 us (0.946)
  the two profiles are of different devices: /device:TPU:1 before, /device:TPU:32 now
where the time goes in v2:
time: 278 us; the launch traced here: 276 us
  Pallas kernels  95.7 us (34%)
  blocking collectives  84.4 us (30%)
  starting transfers between devices  58 us (21%)
  waiting for transfers between devices  27.4 us (10%)
  local copies, waits for them, and re-layouts  4.9 us (2%)
  other arithmetic  4.44 us (2%)
    pallas_call x1, Pallas kernels, attention(): pl.pallas_call(attention_kernel, grid=(1,), out_shape=jax.ShapeDtypeStruc...  79.5 us
    all_to_all x1, blocking collectives, sent_to_all(): lax.all_to_all(jnp.broadcast_to(x[None], (size, *x.shape)), axis, 0, 0, t...  30.6 us
    all_to_all x2, starting transfers between devices, sent_to_all(): lax.all_to_all(jnp.broadcast_to(x[None], (size, *x.shape)), axis, 0, 0, t...  24 us
    all_to_all x1, blocking collectives, body(): landed = lax.all_to_all(blocks, 'tp', 0, 0, tiled=True)  15.9 us
    all_gather x1, blocking collectives, body(): normed = lax.all_gather(own_normed, 'tp', axis=0, tiled=True)  14.6 us
    all_gather x1, blocking collectives, body(): all_queries = lax.all_gather(queries, 'tp', axis=0)  13.5 us
    all_to_all x1, starting transfers between devices, body(): planes = lax.all_to_all(total, 'z', 0, 0, tiled=True)  12 us
    ppermute x3, starting transfers between devices, from_others(): lax.ppermute(x, axis, [((k + ahead) % size, k) for k in range(size)])  11.4 us
  transfers between devices with their start and end apart: 10, of which 8 were waited for; matrix products, arithmetic and copies ran while one was open for 1% of the time, Pallas kernels for 30%

profile of v2, /device:TPU:32, one launch (start us, length us, event | category | flops | bytes accessed | tf_op | source)
XLA Modules:
  0.0 276.4 jit_solution(3699126098257115201)
XLA Ops:
  5.0 15.2 %all-to-all-start = ((bf16[16,16,512]{2,1,0:T(8,128)(2,1)}), bf16[16,16,512]{2,1,0:T(8,128)(2,1)S(1)}, u32[]{:S(2)}, u32[]{:S(2)}) async-start(bf16[16,16,512]{2,1,0:T(8,128)(2,1)} %broadcast_in_dim.12), calls=%async_computation | async-start | bytes 524288 | tf_op jit(solution)/shard_map/all_to_all | solution.py:30
  20.3 14.6 %all_gather.9.normed_ref = bf16[192,2048]{1,0:T(8,128)(2,1)} all-gather(bf16[48,2048]{1,0:T(8,128)(2,1)S(1)} %fusion.5), channel_id=1, replica_groups=mesh['z'=16,'x'=4,'c'=2,'tp'=4] {'tp'}, dimensions={0}, use_global_device_ids=true | all-gather | bytes 983040 | tf_op jit(solution)/shard_map/all_gather | solution.py:509
  34.9 3.2 %all-to-all-done = bf16[16,16,512]{2,1,0:T(8,128)(2,1)S(1)} async-done(((bf16[16,16,512]{2,1,0:T(8,128)(2,1)}), bf16[16,16,512]{2,1,0:T(8,128)(2,1)S(1)}, u32[]{:S(2)}, u32[]{:S(2)}) %all-to-all-start) | async-done | bytes 262176 | tf_op jit(solution)/shard_map/all_to_all | solution.py:30
  39.0 8.8 %all-to-all-start.1 = ((bf16[16,16,1152]{2,1,0:T(8,128)(2,1)}), bf16[16,16,1152]{2,1,0:T(8,128)(2,1)S(1)}, u32[]{:S(2)}, u32[]{:S(2)}) async-start(bf16[16,16,1152]{2,1,0:T(8,128)(2,1)} %broadcast_in_dim.13), calls=%async_computation.1 | async-start | bytes 1179648 | tf_op jit(solution)/shard_map/all_to_all | solution.py:30
  47.8 3.4 %collective-permute-start.2 = (bf16[16,16,512]{2,1,0:T(8,128)(2,1)S(1)}, bf16[16,16,512]{2,1,0:T(8,128)(2,1)S(1)}, u32[]{:S(2)}, u32[]{:S(2)}) collective-permute-start(bf16[16,16,512]{2,1,0:T(8,128)(2,1)S(1)} %all-to-all-done), channel_id=1, source_target_pairs={{24,0},{0,8},{8,16},{16,24},{25,1},{1,9},{9,17},{17,25},{26,2},{2,... | collective-permute-start | bytes 786440 | tf_op jit(solution)/shard_map/ppermute | solution.py:36
  51.2 4.6 %collective-permute-start.1 = (bf16[16,16,512]{2,1,0:T(8,128)(2,1)S(1)}, bf16[16,16,512]{2,1,0:T(8,128)(2,1)S(1)}, u32[]{:S(2)}, u32[]{:S(2)}) collective-permute-start(bf16[16,16,512]{2,1,0:T(8,128)(2,1)S(1)} %all-to-all-done), channel_id=1, source_target_pairs={{16,0},{24,8},{0,16},{8,24},{17,1},{25,9},{1,17},{9,25},{18,2},{26... | collective-permute-start | bytes 786440 | tf_op jit(solution)/shard_map/ppermute | solution.py:36
  55.8 3.3 %collective-permute-start = (bf16[16,16,512]{2,1,0:T(8,128)(2,1)S(1)}, bf16[16,16,512]{2,1,0:T(8,128)(2,1)S(1)}, u32[]{:S(2)}, u32[]{:S(2)}) collective-permute-start(bf16[16,16,512]{2,1,0:T(8,128)(2,1)S(1)} %all-to-all-done), channel_id=1, source_target_pairs={{8,0},{16,8},{24,16},{0,24},{9,1},{17,9},{25,17},{1,25},{10,2},{18... | collective-permute-start | bytes 786440 | tf_op jit(solution)/shard_map/ppermute | solution.py:36
  60.1 3.2 %collective-permute-done.1 = bf16[16,16,512]{2,1,0:T(8,128)(2,1)S(1)} collective-permute-done((bf16[16,16,512]{2,1,0:T(8,128)(2,1)S(1)}, bf16[16,16,512]{2,1,0:T(8,128)(2,1)S(1)}, u32[]{:S(2)}, u32[]{:S(2)}) %collective-permute-start.1) | collective-permute-done | bytes 262176 | tf_op jit(solution)/shard_map/ppermute | solution.py:36
  63.3 2.4 collective-permute-done
  71.3 2.5 shard_map.154
  73.8 13.5 %all-gather = bf16[768,128]{1,0:T(8,128)(2,1)} all-gather(bf16[192,128]{1,0:T(8,128)(2,1)} %shard_map.154), channel_id=2, replica_groups=mesh['z'=16,'x'=4,'c'=2,'tp'=4] {'tp'}, dimensions={0}, use_global_device_ids=true | all-gather | bytes 245760 | tf_op jit(solution)/shard_map/all_gather | solution.py:515
  87.5 30.6 %all_to_all.40.own_ref = bf16[4,16,16,1152]{3,2,1,0:T(8,128)(2,1)S(1)} all-to-all(bf16[4,16,16,1152]{3,2,1,0:T(8,128)(2,1)S(1)} %broadcast_in_dim.15), channel_id=1, replica_groups=mesh['z'=16,'x'=4,'c'=2,'tp'=4] {'x'}, dimensions={0} | all-to-all | bytes 4718592 | tf_op jit(solution)/shard_map/all_to_all | solution.py:30
  120.0 4.6 %collective-permute-done.4.other_ref = bf16[4,16,16,1152]{3,2,1,0:T(8,128)(2,1)} collective-permute-done((bf16[4,16,16,1152]{3,2,1,0:T(8,128)(2,1)S(1)}, bf16[4,16,16,1152]{3,2,1,0:T(8,128)(2,1)}, u32[]{:S(2)}, u32[]{:S(2)}) %collective-permute-start.4) | collective-permute-done | bytes 2359328 | tf_op jit(solution)/shard_map/ppermute | solution.py:520
  124.6 3.8 %shard_map.155.raw_ref = bf16[192,768]{1,0:T(8,128)(2,1)} custom-call(s32[3]{0:T(128)} %pad_add_fusion.place_ref, bf16[4,16,16,1152]{3,2,1,0:T(8,128)(2,1)} %copy-done, bf16[4,16,16,1152]{3,2,1,0:T(8,128)(2,1)} %collective-permute-done.4.other_ref, bf16[192,2048]{1,0:T(8,128)(2,1)} %all_gather.9.normed_ref), custom_call_target="tpu_custom_call" | custom-call | flops 603979776 | bytes 3145728 | tf_op jit(solution)/shard_map/pallas_call | solution.py:92
  128.4 2.9 %recurrence.1 = (f32[2,192,128]{2,1,0:T(8,128)}, bf16[2,192,128]{2,1,0:T(8,128)(2,1)}, bf16[8,48,128]{2,1,0:T(8,128)(2,1)}) custom-call(bf16[192,768]{1,0:T(8,128)(2,1)} %shard_map.155.raw_ref, f32[1,256]{1,0:T(1,128)} %bitcast.25, f32[192,256]{1,0:T(8,128)} %extra_ref.1), custom_call_target="tpu_custom_call" | custom-call | flops 100663296 | bytes 393216 | tf_op jit(solution)/shard_map/recurrence/pallas_call | solution.py:322
  131.4 9.8 %all_to_all.41.pieces_ref = bf16[8,48,128]{2,1,0:T(8,128)(2,1)} all-to-all(bf16[8,48,128]{2,1,0:T(8,128)(2,1)} %get-tuple-element.20), channel_id=1, replica_groups=mesh['z'=16,'x'=4,'c'=2,'tp'=4] {'x','c'}, dimensions={0} | all-to-all | bytes 196608 | tf_op jit(solution)/shard_map/all_to_all | solution.py:526
  142.7 12.0 %all-to-all-start.5 = ((bf16[16,48,128]{2,1,0:T(8,128)(2,1)}), bf16[16,48,128]{2,1,0:T(8,128)(2,1)S(1)}, u32[]{:S(2)}, u32[]{:S(2)}) async-start(bf16[16,48,128]{2,1,0:T(8,128)(2,1)} %plane_total.1), calls=%async_computation.5 | async-start | bytes 393216 | tf_op jit(solution)/shard_map/all_to_all | solution.py:528
  154.8 79.5 %attention.1 = bf16[4,80,768]{2,1,0:T(8,128)(2,1)} custom-call(bf16[4,192,128]{2,1,0:T(8,128)(2,1)} %bitcast.23, bf16[4,16,16,512]{3,2,1,0:T(8,128)(2,1)} %copy-done.1, bf16[4,16,16,512]{3,2,1,0:T(8,128)(2,1)} %copy-done.1, bf16[4,16,16,512]{3,2,1,0:T(8,128)(2,1)} %copy-done.1, bf16[4,16,16,512]{3,2,1,0:T(8,128)(2,1)} %copy-done.3, ...), custom_call_target="tpu_custom_call" | custom-call | flops 19327352832 | bytes 1572864 | tf_op jit(solution)/shard_map/attention/pallas_call | solution.py:240
  234.3 3.5 %all-to-all-start.2 = ((bf16[4,80,768]{2,1,0:T(8,128)(2,1)}), bf16[4,80,768]{2,1,0:T(8,128)(2,1)S(1)}, u32[]{:S(2)}, u32[]{:S(2)}) async-start(bf16[4,80,768]{2,1,0:T(8,128)(2,1)} %attention.1), calls=%async_computation.2 | async-start | bytes 983040 | tf_op jit(solution)/shard_map/all_to_all | solution.py:519
  240.3 6.2 %all-to-all-done.2.parts_ref = bf16[4,80,768]{2,1,0:T(8,128)(2,1)S(1)} async-done(((bf16[4,80,768]{2,1,0:T(8,128)(2,1)}), bf16[4,80,768]{2,1,0:T(8,128)(2,1)S(1)}, u32[]{:S(2)}, u32[]{:S(2)}) %all-to-all-start.2) | async-done | bytes 491552 | tf_op jit(solution)/shard_map/all_to_all | solution.py:519
  246.5 3.3 %all-to-all-start.6 = ((bf16[8,32,128]{2,1,0:T(8,128)(2,1)}), bf16[8,32,128]{2,1,0:T(8,128)(2,1)S(1)}, u32[]{:S(2)}, u32[]{:S(2)}) async-start(bf16[8,32,128]{2,1,0:T(8,128)(2,1)} %states_before.1), calls=%async_computation.6 | async-start | bytes 131072 | tf_op jit(solution)/shard_map/all_to_all | solution.py:531
  250.5 4.8 %all-to-all-done.6 = bf16[8,32,128]{2,1,0:T(8,128)(2,1)S(1)} async-done(((bf16[8,32,128]{2,1,0:T(8,128)(2,1)}), bf16[8,32,128]{2,1,0:T(8,128)(2,1)S(1)}, u32[]{:S(2)}, u32[]{:S(2)}) %all-to-all-start.6) | async-done | bytes 65568 | tf_op jit(solution)/shard_map/all_to_all | solution.py:531
  256.0 3.7 %output_partial.1 = bf16[192,2048]{1,0:T(8,128)(2,1)} custom-call(s32[3]{0:T(128)} %pad_add_fusion.place_ref, f32[2]{0:T(128)} %second_ref.1, bf16[4,80,768]{2,1,0:T(8,128)(2,1)} %copy-done.2, f32[64,1]{1,0:T(8,128)} %copy.18.attn_gain_ref, f32[2,192,128]{2,1,0:T(8,128)} %get-tuple-element.18.local_ref, bf16[2,192,128]{2,1,0:T(8,128)(2,1)} %get-tuple-element.19.lifted_ref, ...), custom_call_target="tpu_custom_call" | custom-call | flops 301989888 | bytes 1572864 | tf_op jit(solution)/shard_map/output_partial/pallas_call | solution.py:456
  259.6 15.9 %all_to_all.42 = bf16[4,48,2048]{2,1,0:T(8,128)(2,1)S(1)} all-to-all(bf16[4,48,2048]{2,1,0:T(8,128)(2,1)} %bitcast.16), channel_id=1, replica_groups=mesh['z'=16,'x'=4,'c'=2,'tp'=4] {'tp'}, dimensions={0} | all-to-all | bytes 1572864 | tf_op jit(solution)/shard_map/all_to_all | solution.py:547
  (53 shorter events, 20.7 us)
Async XLA Ops:
  0.0 20.2 %copy-start.7 = (bf16[16,256]{1,0:T(8,128)(2,1)S(1)}, bf16[16,256]{1,0:T(8,128)(2,1)}, u32[]{:S(2)}) copy-start(bf16[16,256]{1,0:T(8,128)(2,1)} %param.21) | copy-start | bytes 24580
  0.0 20.2 %copy-start.8 = (bf16[16,256]{1,0:T(8,128)(2,1)S(1)}, bf16[16,256]{1,0:T(8,128)(2,1)}, u32[]{:S(2)}) copy-start(bf16[16,256]{1,0:T(8,128)(2,1)} %param.22) | copy-start | bytes 24580
  0.0 20.2 %copy-start.9 = (bf16[16,256]{1,0:T(8,128)(2,1)S(1)}, bf16[16,256]{1,0:T(8,128)(2,1)}, u32[]{:S(2)}) copy-start(bf16[16,256]{1,0:T(8,128)(2,1)} %param.23) | copy-start | bytes 24580
  0.0 20.3 %copy-start.11 = (bf16[16,128]{1,0:T(8,128)(2,1)S(1)}, bf16[16,128]{1,0:T(8,128)(2,1)}, u32[]{:S(2)}) copy-start(bf16[16,128]{1,0:T(8,128)(2,1)} %param.24) | copy-start | bytes 12292
  0.0 20.3 %copy-start.10 = (bf16[16,256]{1,0:T(8,128)(2,1)S(1)}, bf16[16,256]{1,0:T(8,128)(2,1)}, u32[]{:S(2)}) copy-start(bf16[16,256]{1,0:T(8,128)(2,1)} %param.25) | copy-start | bytes 24580
  5.0 33.1 %all-to-all-start = ((bf16[16,16,512]{2,1,0:T(8,128)(2,1)}), bf16[16,16,512]{2,1,0:T(8,128)(2,1)S(1)}, u32[]{:S(2)}, u32[]{:S(2)}) async-start(bf16[16,16,512]{2,1,0:T(8,128)(2,1)} %broadcast_in_dim.12), calls=%async_computation | async-start | bytes 524288 | tf_op jit(solution)/shard_map/all_to_all | solution.py:30
  39.0 48.3 %all-to-all-start.1 = ((bf16[16,16,1152]{2,1,0:T(8,128)(2,1)}), bf16[16,16,1152]{2,1,0:T(8,128)(2,1)S(1)}, u32[]{:S(2)}, u32[]{:S(2)}) async-start(bf16[16,16,1152]{2,1,0:T(8,128)(2,1)} %broadcast_in_dim.13), calls=%async_computation.1 | async-start | bytes 1179648 | tf_op jit(solution)/shard_map/all_to_all | solution.py:30
  47.8 12.3 %collective-permute-start.2 = (bf16[16,16,512]{2,1,0:T(8,128)(2,1)S(1)}, bf16[16,16,512]{2,1,0:T(8,128)(2,1)S(1)}, u32[]{:S(2)}, u32[]{:S(2)}) collective-permute-start(bf16[16,16,512]{2,1,0:T(8,128)(2,1)S(1)} %all-to-all-done), channel_id=1, source_target_pairs={{24,0},{0,8},{8,16},{16,24},{25,1},{1,9},{9,17},{17,25},{26,2},{2,... | collective-permute-start | bytes 786440 | tf_op jit(solution)/shard_map/ppermute | solution.py:36
  51.2 12.1 %collective-permute-start.1 = (bf16[16,16,512]{2,1,0:T(8,128)(2,1)S(1)}, bf16[16,16,512]{2,1,0:T(8,128)(2,1)S(1)}, u32[]{:S(2)}, u32[]{:S(2)}) collective-permute-start(bf16[16,16,512]{2,1,0:T(8,128)(2,1)S(1)} %all-to-all-done), channel_id=1, source_target_pairs={{16,0},{24,8},{0,16},{8,24},{17,1},{25,9},{1,17},{9,25},{18,2},{26... | collective-permute-start | bytes 786440 | tf_op jit(solution)/shard_map/ppermute | solution.py:36
  55.8 9.8 %collective-permute-start = (bf16[16,16,512]{2,1,0:T(8,128)(2,1)S(1)}, bf16[16,16,512]{2,1,0:T(8,128)(2,1)S(1)}, u32[]{:S(2)}, u32[]{:S(2)}) collective-permute-start(bf16[16,16,512]{2,1,0:T(8,128)(2,1)S(1)} %all-to-all-done), channel_id=1, source_target_pairs={{8,0},{16,8},{24,16},{0,24},{9,1},{17,9},{25,17},{1,25},{10,2},{18... | collective-permute-start | bytes 786440 | tf_op jit(solution)/shard_map/ppermute | solution.py:36
  65.8 4.6 %copy-start.1 = (bf16[4,16,16,512]{3,2,1,0:T(8,128)(2,1)}, bf16[4,16,16,512]{3,2,1,0:T(8,128)(2,1)S(1)}, u32[]{:S(2)}) copy-start(bf16[4,16,16,512]{3,2,1,0:T(8,128)(2,1)S(1)} %pad_maximum_fusion.own_ref.refs_0_.refs_1_.refs_2_) | copy-start | bytes 3145732
  65.8 4.6 %collective-permute-start.3 = (bf16[4,16,16,512]{3,2,1,0:T(8,128)(2,1)S(1)}, bf16[4,16,16,512]{3,2,1,0:T(8,128)(2,1)S(1)}, u32[]{:S(2)}, u32[]{:S(2)}) collective-permute-start(bf16[4,16,16,512]{3,2,1,0:T(8,128)(2,1)S(1)} %pad_maximum_fusion.own_ref.refs_0_.refs_1_.refs_2_), channel_id=1, source_target_pairs={{0,4},{4,0},{1,5},{5,1},{2,6},{6,2},{3,7},{7,3},{8,12},{12,8},{9,1... | collective-permute-start | bytes 3145736 | tf_op jit(solution)/shard_map/ppermute | solution.py:513
  70.3 1.0 copy-start.3
  118.1 6.6 %copy-start = (bf16[4,16,16,1152]{3,2,1,0:T(8,128)(2,1)}, bf16[4,16,16,1152]{3,2,1,0:T(8,128)(2,1)S(1)}, u32[]{:S(2)}) copy-start(bf16[4,16,16,1152]{3,2,1,0:T(8,128)(2,1)S(1)} %all_to_all.40.own_ref) | copy-start | bytes 7077892
  118.1 6.5 %collective-permute-start.4 = (bf16[4,16,16,1152]{3,2,1,0:T(8,128)(2,1)S(1)}, bf16[4,16,16,1152]{3,2,1,0:T(8,128)(2,1)}, u32[]{:S(2)}, u32[]{:S(2)}) collective-permute-start(bf16[4,16,16,1152]{3,2,1,0:T(8,128)(2,1)S(1)} %all_to_all.40.own_ref), channel_id=1, source_target_pairs={{0,4},{4,0},{1,5},{5,1},{2,6},{6,2},{3,7},{7,3},{8,12},{12,8},{9,1... | collective-permute-start | bytes 7077896 | tf_op jit(solution)/shard_map/ppermute | solution.py:520
  142.7 91.6 %all-to-all-start.5 = ((bf16[16,48,128]{2,1,0:T(8,128)(2,1)}), bf16[16,48,128]{2,1,0:T(8,128)(2,1)S(1)}, u32[]{:S(2)}, u32[]{:S(2)}) async-start(bf16[16,48,128]{2,1,0:T(8,128)(2,1)} %plane_total.1), calls=%async_computation.5 | async-start | bytes 393216 | tf_op jit(solution)/shard_map/all_to_all | solution.py:528
  154.8 83.0 %copy-start.6 = (f32[2,128,128]{2,1,0:T(8,128)S(1)}, f32[2,128,128]{2,1,0:T(8,128)}, u32[]{:S(2)}) copy-start(f32[2,128,128]{2,1,0:T(8,128)} %param.31) | copy-start | bytes 393220
  154.8 95.1 %copy-start.12 = (f32[64]{0:T(128)S(1)}, f32[64]{0:T(128)}, u32[]{:S(2)}) copy-start(f32[64]{0:T(128)} %param.26) | copy-start | bytes 772
  234.3 4.2 %copy-start.4 = (bf16[16,48,128]{2,1,0:T(8,128)(2,1)}, bf16[16,48,128]{2,1,0:T(8,128)(2,1)S(1)}, u32[]{:S(2)}) copy-start(bf16[16,48,128]{2,1,0:T(8,128)(2,1)S(1)} %all-to-all-done.5.planes_ref) | copy-start | bytes 589828
  234.3 12.1 %all-to-all-start.2 = ((bf16[4,80,768]{2,1,0:T(8,128)(2,1)}), bf16[4,80,768]{2,1,0:T(8,128)(2,1)S(1)}, u32[]{:S(2)}, u32[]{:S(2)}) async-start(bf16[4,80,768]{2,1,0:T(8,128)(2,1)} %attention.1), calls=%async_computation.2 | async-start | bytes 983040 | tf_op jit(solution)/shard_map/all_to_all | solution.py:519
  246.5 8.9 %copy-start.2 = (bf16[4,80,768]{2,1,0:T(8,128)(2,1)}, bf16[4,80,768]{2,1,0:T(8,128)(2,1)S(1)}, u32[]{:S(2)}) copy-start(bf16[4,80,768]{2,1,0:T(8,128)(2,1)S(1)} %all-to-all-done.2.parts_ref) | copy-start | bytes 1474564
  246.5 8.9 %all-to-all-start.6 = ((bf16[8,32,128]{2,1,0:T(8,128)(2,1)}), bf16[8,32,128]{2,1,0:T(8,128)(2,1)S(1)}, u32[]{:S(2)}, u32[]{:S(2)}) async-start(bf16[8,32,128]{2,1,0:T(8,128)(2,1)} %states_before.1), calls=%async_computation.6 | async-start | bytes 131072 | tf_op jit(solution)/shard_map/all_to_all | solution.py:531
  255.4 0.6 copy-start.5
